TPU v7x, 32 devices: a whole 2x2x4 slice. The times are simulated.
32 devices in a mesh: sp: 4 (over z), fs: 4 (over y, x), tp: 2 (over core).
Axes of the slice: x: 2, y: 2, z: 4, core: 2. Of those that a mesh axis runs over, the one named last changes fastest.
Arguments:
- tokens: bfloat16 [4, 1024, 2048], P('fs', 'sp'), may hold values from -6 to 6
- norm_gain: float32 [2048], replicated, may hold values from 0.1 to 1.9
- pool_input: bfloat16 [2048, 2048], P(('sp', 'fs'), 'tp'), may hold values from -0.125 to 0.125
- query_weight: bfloat16 [2048, 2048], P(('sp', 'fs'), 'tp'), may hold values from -20 to 20
- key_weight: bfloat16 [2048, 2048], P(('sp', 'fs'), 'tp'), may hold values from -1 to 1
- value_weight: bfloat16 [2048, 2048], P(('sp', 'fs'), 'tp'), may hold values from -0.125 to 0.125
- pool_map: bfloat16 [8, 256, 256], P('tp'), may hold values from -0.375 to 0.375
- pool_scale: float32 [2048], P('tp'), may hold values from 0.1 to 1.9
- head_gain: float32 [256], replicated, may hold values from 0.1 to 1.9
- diff_lambda: float32 [8], replicated, may hold values from 0.3 to 0.8
- out_pool: bfloat16 [2048, 2048], P('tp', ('sp', 'fs')), may hold values from -0.09375 to 0.09375
- out_heads: bfloat16 [2048, 2048], P('tp', ('sp', 'fs')), may hold values from -0.09375 to 0.09375
Outputs:
- layer_out: bfloat16 [4, 1024, 2048], P('fs', 'sp', 'tp')
All inputs are finite; a program needn't handle non-finite values.
Results may differ from a plain program's by a relative error of at most 0.018.
Values may be sent and summed in bfloat16 or wider, within the bound.
A program may use at most 64 MiB of HBM per device.

v0:
```python
import math

import jax
import jax.numpy as jnp
from jax import lax
from jax.experimental import pallas as pl
from jax.experimental.pallas import tpu as pltpu
from jax.sharding import PartitionSpec as P

HEAD_DIM = 128
GROUP_DIM = 256


THETA = 500000.0
HEAD_SCALE = 0.8
NORM_EPS = 1e-06
HEAD_EPS = 1e-05


def from_behind(value, axis, steps):
    count = lax.axis_size(axis)
    first, last = (max(0, -steps), min(count, count - steps))
    return lax.ppermute(value, axis, [(source, source + steps) for source in range(first, last)])


def rotate(tensor, positions):
    half = HEAD_DIM // 2
    freqs = 1.0 / THETA ** (jnp.arange(half, dtype=jnp.float32) * 2.0 / HEAD_DIM)
    angles = positions[:, None] * freqs[None, :]
    cosine = jnp.cos(angles)[:, None, None, :]
    sine = jnp.sin(angles)[:, None, None, :]
    floated = tensor.astype(jnp.float32)
    first = floated[..., :half]
    second = floated[..., half:]
    turned = jnp.concatenate([first * cosine - second * sine, second * cosine + first * sine], -1)
    return turned.astype(jnp.bfloat16)


def local(
    tokens,
    norm_gain,
    pool_input,
    query_weight,
    key_weight,
    value_weight,
    pool_map,
    pool_scale,
    head_gain,
    diff_lambda,
    out_pool,
    out_heads,
):
    out_local = jnp.concatenate([out_pool, out_heads], 0)
    row_count = tokens.shape[1]
    floated = tokens[0].astype(jnp.float32)
    normed = (
        floated * lax.rsqrt(jnp.mean(floated * floated, -1, keepdims=True) + NORM_EPS) * norm_gain
    ).astype(jnp.bfloat16)
    fragments = (
        lax.all_gather(pool_input, ("sp", "fs"), axis=0, tiled=True),
        lax.all_gather(query_weight, ("sp", "fs"), axis=0, tiled=True),
        lax.all_gather(key_weight, ("sp", "fs"), axis=0, tiled=True),
        lax.all_gather(value_weight, ("sp", "fs"), axis=0, tiled=True),
    )
    projected = tuple(
        (jnp.dot(normed, fragment, preferred_element_type=jnp.float32) for fragment in fragments)
    )
    pool_in, queries, keys_flat, values_flat = [
        product.astype(jnp.bfloat16) for product in projected
    ]
    head_count = values_flat.shape[1] // (2 * HEAD_DIM)
    tp_index = lax.axis_index("tp")
    sp_index = lax.axis_index("sp")
    query_pos = sp_index * row_count + jnp.arange(row_count, dtype=jnp.int32)
    positions = query_pos.astype(jnp.float32)
    queries = rotate(queries.reshape(row_count, head_count, 2, HEAD_DIM), positions)
    keys_flat = rotate(keys_flat.reshape(row_count, head_count, 2, HEAD_DIM), positions).reshape(
        row_count, head_count * 2 * HEAD_DIM
    )
    lambdas = lax.dynamic_slice_in_dim(diff_lambda, tp_index * head_count, head_count, 0)

    def online_step(state, key_rows, value_rows, key_offset):
        largest, summed, accum = state
        width = key_rows.shape[0]
        shaped = key_rows.reshape(width, head_count, 2, HEAD_DIM)
        scores = jnp.einsum(
            "qhcd,khcd->chqk", queries, shaped, preferred_element_type=jnp.float32
        ) * HEAD_DIM ** (-0.5)
        key_pos = key_offset + jnp.arange(width, dtype=jnp.int32)
        scores = jnp.where(query_pos[:, None] >= key_pos[None, :], scores, -jnp.inf)
        newest = jnp.maximum(largest, jnp.max(scores, -1))
        anchor = jnp.where(jnp.isfinite(newest), newest, 0.0)
        rescale = jnp.exp(largest - anchor)
        expons = jnp.exp(scores - anchor[..., None])
        summed = summed * rescale + jnp.sum(expons, -1)
        value_shaped = value_rows.reshape(width, head_count, 2 * HEAD_DIM)
        added = jnp.einsum(
            "chqk,khe->chqe",
            expons.astype(jnp.bfloat16),
            value_shaped,
            preferred_element_type=jnp.float32,
        )
        accum = accum * rescale[..., None] + added
        return (newest, summed, accum)

    start_state = (
        jnp.full((2, head_count, row_count), -jnp.inf, jnp.float32),
        jnp.zeros((2, head_count, row_count), jnp.float32),
        jnp.zeros((2, head_count, row_count, 2 * HEAD_DIM), jnp.float32),
    )
    fragments = (
        lax.all_gather(keys_flat, "sp", axis=0, tiled=True),
        lax.all_gather(values_flat, "sp", axis=0, tiled=True),
    )
    span = math.gcd(fragments[0].shape[0], 1024)

    def inner_step(index, inner_state):
        key_rows = lax.dynamic_slice_in_dim(fragments[0], index * span, span, 0)
        value_rows = lax.dynamic_slice_in_dim(fragments[1], index * span, span, 0)
        return online_step(inner_state, key_rows, value_rows, index * span)

    final_state = lax.fori_loop(0, fragments[0].shape[0] // span, inner_step, start_state)
    summed_final = final_state[1]
    accum_final = final_state[2]
    heads_raw = (
        accum_final[0] / summed_final[0][..., None]
        - lambdas[:, None, None] * accum_final[1] / summed_final[1][..., None]
    )
    heads_raw = jnp.moveaxis(heads_raw, 0, 1)
    attn = (
        (
            heads_raw
            * lax.rsqrt(jnp.mean(heads_raw * heads_raw, -1, keepdims=True) + HEAD_EPS)
            * head_gain
            * HEAD_SCALE
        )
        .astype(jnp.bfloat16)
        .reshape(row_count, head_count * 2 * HEAD_DIM)
    )
    reach = 15
    rim_rows = from_behind(pool_in[row_count - reach :], "sp", 1)
    extended = jnp.concatenate([rim_rows, pool_in], 0).astype(jnp.float32)
    pair_sums = extended[1:] + extended[:-1]
    quad_sums = pair_sums[2:] + pair_sums[:-2]
    octet_sums = quad_sums[4:] + quad_sums[:-4]
    sixteen_sums = octet_sums[8:] + octet_sums[:-8]
    group_count = pool_in.shape[1] // GROUP_DIM
    stacked = jnp.stack(
        [
            pair_sums[14 : 14 + row_count],
            quad_sums[12 : 12 + row_count],
            octet_sums[8 : 8 + row_count],
            sixteen_sums,
        ],
        0,
    ).reshape(4, row_count, group_count, GROUP_DIM)
    levels = (tp_index * group_count + jnp.arange(group_count, dtype=jnp.int32)) % 4
    picked = jnp.sum(
        jnp.where(
            levels[None, None, :, None] == jnp.arange(4, dtype=jnp.int32)[:, None, None, None],
            stacked,
            0.0,
        ),
        0,
    )
    windows = 2 ** (1 + levels)
    counts = jnp.minimum(query_pos[:, None] + 1, windows[None, :]).astype(jnp.float32)
    window_mean = picked / counts[:, :, None]
    grouped = pool_in.reshape(row_count, group_count, GROUP_DIM).astype(jnp.float32)
    pool_mixed = (window_mean - grouped).astype(jnp.bfloat16)
    pooled = (
        (
            jnp.einsum("tgc,gce->tge", pool_mixed, pool_map, preferred_element_type=jnp.float32)
            * pool_scale.reshape(group_count, GROUP_DIM)
        )
        .astype(jnp.bfloat16)
        .reshape(row_count, group_count * GROUP_DIM)
    )
    branches = jnp.concatenate([pooled, attn], 1)
    partial_value = jnp.dot(
        branches,
        lax.all_gather(out_local, ("sp", "fs"), axis=1, tiled=True),
        preferred_element_type=jnp.float32,
    )
    layer_out = lax.psum_scatter(
        partial_value.astype(jnp.bfloat16), "tp", scatter_dimension=1, tiled=True
    )
    return layer_out[None]


MESH = pl.DeviceIdType.MESH
PIECES = 4
PARTS = 2

def fused_kernel(
    places,
    groups,
    tokens_ref,
    norm_gain_ref,
    freqs_ref,
    pool_ref,
    query_ref,
    key_ref,
    value_ref,
    map_ref,
    scale_ref,
    gain_ref,
    lambda_ref,
    out_pool_ref,
    out_heads_ref,
    out_ref,
    normed_ref,
    cos_ref,
    sin_ref,
    rows_all,
    weights,
    outs,
    queries,
    keys,
    values,
    pools,
    to_mate,
    from_mate,
    to_peer,
    from_peer,
    merging,
    final,
    *sems,
):
    (
        own_sem,
        in_local,
        in_z_send,
        in_z_recv,
        in_n_send,
        in_n_recv,
        in_f_send,
        in_f_recv,
        out_local,
        out_z_send,
        out_z_recv,
        out_n_send,
        out_n_recv,
        out_f_send,
        out_f_recv,
        right_send,
        right_recv,
        left_send,
        left_recv,
        mate_send,
        mate_recv,
        half_send,
        half_recv,
        peer_send,
        peer_recv,
        merge_send,
        merge_recv,
    ) = sems
    z = lax.axis_index("sp")
    f = lax.axis_index("fs")
    c = lax.axis_index("tp")
    fx = f + 1 - 2 * lax.rem(f, 2)
    fy = lax.rem(f + 2, groups)
    mate = 1 - c
    half_rows = tokens_ref.shape[0] // 2
    row_count = 2 * half_rows
    depth = pool_ref.shape[0]
    width = GROUP_DIM
    out_width = out_pool_ref.shape[1]
    half_out = out_ref.shape[1]

    barrier = pltpu.get_barrier_semaphore()
    partners = [{"sp": lax.rem(z + d, places)} for d in range(1, places)]
    partners += [{"fs": fx}, {"fs": fy}, {"tp": mate}]
    for partner in partners:
        pl.semaphore_signal(barrier, inc=1, device_id=partner, device_id_type=MESH)
    pl.semaphore_wait(barrier, len(partners))

    def remote(source, target, send, recv, device):
        return pltpu.make_async_remote_copy(
            src_ref=source,
            dst_ref=target,
            send_sem=send,
            recv_sem=recv,
            device_id=device,
            device_id_type=MESH,
        )

    def block(index, size):
        return pl.ds(pl.multiple_of(index * size, size), size)

    class Gather:
        def __init__(self, sources, cut, view, group):
            self.sources, self.cut, self.view = sources, cut, view
            self.count = len(sources)
            (
                self.local,
                self.z_send,
                self.z_recv,
                self.n_send,
                self.n_recv,
                self.f_send,
                self.f_recv,
            ) = group
            self.low = (0, self.count // 2)
            self.high = (self.count // 2, self.count - self.count // 2)

        def own(self, m):
            return pltpu.make_async_copy(
                self.cut(self.sources[m], z), self.view(z, f, m, 1).at[0], self.local.at[m]
            )

        def across(self, d, m):
            to = lax.rem(z + d, places)
            return remote(
                self.cut(self.sources[m], to),
                self.view(z, f, m, 1).at[0],
                self.z_send.at[d, m],
                self.z_recv.at[d, m],
                {"sp": to},
            )

        def arrive(self, d, m):
            view = self.view(lax.rem(z + places - d, places), f, m, 1).at[0]
            return remote(
                view,
                view,
                self.z_send.at[d, m],
                self.z_recv.at[d, m],
                {"sp": lax.rem(z + places - d, places)},
            )

        def near(self, d, side, column, half):
            start, size = (self.low, self.high)[half]
            view = self.view(lax.rem(z + places - d, places), column, start, size)
            return remote(
                view,
                view,
                self.n_send.at[side, 2 * d + half],
                self.n_recv.at[side, 2 * d + half],
                {"fs": (fx, fy)[side]},
            )

        def forward(self, d, side, column):
            start, size = (self.high, self.low)[side]
            view = self.view(lax.rem(z + places - d, places), column, start, size)
            return remote(
                view,
                view,
                self.f_send.at[side, d],
                self.f_recv.at[side, d],
                {"fs": (fx, fy)[side]},
            )

        def start(self):
            for m in range(self.count):
                self.own(m).start()
            for d in range(1, places):
                for m in range(self.count):
                    self.across(d, m).start()

        def first(self, d):
            for m in range(self.count):
                if d == 0:
                    self.own(m).wait()
                else:
                    self.arrive(d, m).wait_recv()
            for order in range(2):
                for side in range(2):
                    self.near(d, side, f, side ^ order).start()

        def second(self, d):
            self.near(d, 0, fx, 0).wait_recv()
            self.forward(d, 1, fx).start()
            self.near(d, 1, fy, 1).wait_recv()
            self.forward(d, 0, fy).start()

        def third(self, d):
            diagonal = lax.rem(fx + 2, groups)
            for side in range(2):
                self.forward(d, side, diagonal).wait_recv()
            self.near(d, 0, fx, 1).wait_recv()
            self.near(d, 1, fy, 0).wait_recv()

        def drain(self):
            for d in range(places):
                for m in range(self.count):
                    if d > 0:
                        self.across(d, m).wait_send()
                for side in range(2):
                    for half in range(2):
                        self.near(d, side, f, half).wait_send()
                self.forward(d, 1, fx).wait_send()
                self.forward(d, 0, fy).wait_send()

    inward = Gather(
        (pool_ref, query_ref, key_ref, value_ref),
        lambda ref, to: ref.at[:, block(to, width)],
        lambda zz, ff, m, n: weights.at[pl.ds(m, n), block(zz * groups + ff, depth), :],
        (in_local, in_z_send, in_z_recv, in_n_send, in_n_recv, in_f_send, in_f_recv),
    )
    outward = Gather(
        (out_pool_ref, out_heads_ref),
        lambda ref, to: ref.at[block(to, width), :],
        lambda zz, ff, m, n: outs.at[pl.ds(m, n), :, block(zz * groups + ff, out_width)],
        (out_local, out_z_send, out_z_recv, out_n_send, out_n_recv, out_f_send, out_f_recv),
    )

    piece_rows = half_rows // PIECES

    def chunk(zz, side, p):
        return rows_all.at[block((2 * zz + side) * PIECES + p, piece_rows), :]

    def right(k, p):
        view = chunk(z - k, c, p)
        return remote(view, view, right_send.at[k, p], right_recv.at[k + 1, p], {"sp": z + 1})

    def from_left(k, p):
        view = chunk(z - k, c, p)
        return remote(view, view, right_send.at[k, p], right_recv.at[k, p], {"sp": z - 1})

    def left(k, p):
        view = chunk(z + k, c, p)
        return remote(view, view, left_send.at[k, p], left_recv.at[k + 1, p], {"sp": z - 1})

    def from_right(k, p):
        view = chunk(z + k, c, p)
        return remote(view, view, left_send.at[k, p], left_recv.at[k, p], {"sp": z + 1})

    def share(slot, zz, side, p):
        view = chunk(zz, side, p)
        return remote(view, view, mate_send.at[slot, p], mate_recv.at[slot, p], {"tp": mate})

    own_rows = pltpu.make_async_copy(
        normed_ref, rows_all.at[block(2 * z + c, half_rows), :], own_sem
    )
    inward.start()
    outward.start()
    floated = tokens_ref[pl.ds(pl.multiple_of(c * half_rows, 16), half_rows), :].astype(
        jnp.float32
    )
    normed_ref[...] = (
        floated
        * lax.rsqrt(jnp.mean(floated * floated, -1, keepdims=True) + NORM_EPS)
        * norm_gain_ref[...]
    ).astype(jnp.bfloat16)
    own_rows.start()
    own_rows.wait()

    @pl.when(z < places - 1)
    def _():
        for p in range(PIECES):
            right(0, p).start()

    @pl.when(z > 0)
    def _():
        for p in range(PIECES):
            left(0, p).start()

    for p in range(PIECES):
        share(0, z, c, p).start()

    def tokens_step(k):
        for p in range(PIECES):

            @pl.when(z >= k)
            def _():
                from_left(k, p).wait_recv()

                @pl.when(z < places - 1)
                def _():
                    right(k, p).start()

                share(k, z - k, c, p).start()

            @pl.when(z + k < places)
            def _():
                from_right(k, p).wait_recv()

                @pl.when(z > 0)
                def _():
                    left(k, p).start()

                share(places - 1 + k, z + k, c, p).start()

    pools[0:16, :] = jnp.zeros((16, width), jnp.bfloat16)
    inward.first(0)

    def table(index, carry):
        rows = block(index, row_count)
        half = HEAD_DIM // 2
        count = (
            index * row_count + lax.broadcasted_iota(jnp.int32, (row_count, HEAD_DIM), 0)
        ).astype(jnp.float32)
        lane = lax.broadcasted_iota(jnp.int32, (row_count, HEAD_DIM), 1)
        angles = count * freqs_ref[...]
        cos_ref[rows, :] = jnp.cos(angles)
        sine = jnp.sin(angles)
        sin_ref[rows, :] = jnp.where(lane < half, -sine, sine)
        return carry

    lax.fori_loop(0, places, table, 0)
    for d in range(1, places):
        inward.first(d)
        inward.second(d - 1)
    outward.first(0)
    inward.second(places - 1)
    for d in range(1, places):
        outward.first(d)
        if d > 1:
            outward.second(d - 2)
    tokens_step(1)
    for d in (places - 2, places - 1):
        outward.second(d)
    for k in range(2, places):
        tokens_step(k)
    for d in range(places):
        inward.third(d)

    for p in range(PIECES):
        share(0, z, mate, p).wait_recv()
        for k in range(1, places):

            @pl.when(z >= k)
            def _():
                share(k, z - k, mate, p).wait_recv()

            @pl.when(z + k < places)
            def _():
                share(places - 1 + k, z + k, mate, p).wait_recv()

    def turned(raw, cosine, sine):
        floated = raw.astype(jnp.float32)
        return (floated * cosine + pltpu.roll(floated, HEAD_DIM // 2, 1) * sine).astype(
            jnp.bfloat16
        )

    def project(index, carry):
        rows = block(index, row_count)
        normed = rows_all[rows, :]
        cosine = cos_ref[rows, :]
        sine = sin_ref[rows, :]

        def product(m):
            return jnp.dot(normed, weights[m], preferred_element_type=jnp.float32).astype(
                jnp.bfloat16
            )

        pools[pl.ds(pl.multiple_of(index * row_count + 16, 16), row_count), :] = product(0)
        raw = product(1)
        for m in range(2):
            part = slice(m * HEAD_DIM, (m + 1) * HEAD_DIM)
            queries[rows, part] = turned(raw[:, part], cosine, sine)
        raw = product(2)
        for m in range(2):
            part = slice(m * HEAD_DIM, (m + 1) * HEAD_DIM)
            keys[rows, part] = turned(raw[:, part], cosine, sine)
        values[rows, :] = product(3)
        return carry

    lax.fori_loop(0, places, project, 0)
    for d in range(places):
        outward.third(d)

    level = lax.rem(c * map_ref.shape[0] + z, 4)
    window = jnp.where(
        level == 0, 2, jnp.where(level == 1, 4, jnp.where(level == 2, 8, 16))
    )
    head_lambda = lambda_ref[c * map_ref.shape[0] + z]
    length = places * row_count

    part_rows = row_count // PARTS

    def to_sibling(step):
        return remote(
            to_mate.at[step],
            from_mate.at[step],
            half_send.at[step],
            half_recv.at[step],
            {"tp": mate},
        )

    outer = (z == 0) | (z == places - 1)
    pair = z + 1 - 2 * lax.rem(z, 2)
    far = jnp.where(z < 2, places - 1, 0)
    near = jnp.where(z < 2, 2, 1)

    def to_inner(role, to, h):
        return remote(
            to_peer.at[to * PARTS + h],
            merging.at[role * PARTS + h],
            merge_send.at[role * PARTS + h],
            merge_recv.at[role * PARTS + h],
            {"sp": pair},
        )

    def to_place(role, to, h):
        return remote(
            to_peer.at[to * PARTS + h],
            from_peer.at[h],
            peer_send.at[role * PARTS + h],
            peer_recv.at[h],
            {"sp": to},
        )

    def to_pair(h):
        return remote(
            to_peer.at[pair * PARTS + h],
            from_peer.at[PARTS + h],
            peer_send.at[2 * PARTS + h],
            peer_recv.at[PARTS + h],
            {"sp": pair},
        )

    def compute(step, carry):
        turn = step // PARTS
        h = lax.rem(step, PARTS)
        role = jnp.where((turn == 3) | outer, turn, lax.rem(turn + 2, 3))
        to = jnp.where(role == 0, far, jnp.where(role == 1, near, jnp.where(role == 2, pair, z)))
        slot = to * PARTS + h
        rows = block(slot, part_rows)
        query_pos = slot * part_rows + lax.broadcasted_iota(jnp.int32, (part_rows, length), 0)
        key_pos = lax.broadcasted_iota(jnp.int32, (part_rows, length), 1)
        seen = query_pos >= key_pos
        mapped = []
        for m in range(2):
            part = slice(m * HEAD_DIM, (m + 1) * HEAD_DIM)
            scores = lax.dot_general(
                queries[rows, part],
                keys[:, part],
                (((1,), (1,)), ((), ())),
                preferred_element_type=jnp.float32,
            ) * HEAD_DIM ** (-0.5)
            scores = jnp.where(seen, scores, -jnp.inf)
            expons = jnp.exp(scores - jnp.max(scores, -1, keepdims=True))
            totals = jnp.sum(expons, -1, keepdims=True)
            mapped.append(
                jnp.dot(
                    expons.astype(jnp.bfloat16), values[...], preferred_element_type=jnp.float32
                )
                / totals
            )
        raw = mapped[0] - head_lambda * mapped[1]
        attn = (
            raw
            * lax.rsqrt(jnp.mean(raw * raw, -1, keepdims=True) + HEAD_EPS)
            * gain_ref[...]
            * HEAD_SCALE
        ).astype(jnp.bfloat16)
        extended = pools[
            pl.ds(pl.multiple_of(slot * part_rows, 16), part_rows + 16), :
        ].astype(jnp.float32)
        picked = extended + pltpu.roll(extended, 1, 0)
        sums = picked
        for shift in (2, 4, 8):
            sums = sums + pltpu.roll(sums, shift, 0)
            picked = lax.select_n(window >= 2 * shift, picked, sums)
        places_of = slot * part_rows + lax.broadcasted_iota(jnp.int32, (part_rows, 1), 0)
        counts = jnp.minimum(places_of + 1, window).astype(jnp.float32)
        mixed = (picked[16:] / counts - extended[16:]).astype(jnp.bfloat16)
        pooled = (
            jnp.dot(mixed, map_ref[z], preferred_element_type=jnp.float32) * scale_ref[z]
        ).astype(jnp.bfloat16)

        def partial_of(side):
            columns = block(side, half_out)
            return jnp.dot(
                pooled, outs[0, :, columns], preferred_element_type=jnp.float32
            ) + jnp.dot(attn, outs[1, :, columns], preferred_element_type=jnp.float32)

        to_mate[step] = partial_of(mate).astype(jnp.bfloat16)
        to_sibling(step).start()
        mine = partial_of(c)
        to_sibling(step).wait_recv()
        summed = mine + from_mate[step].astype(jnp.float32)

        @pl.when((role < 2) & outer)
        def _():
            to_peer[slot] = summed.astype(jnp.bfloat16)
            to_inner(role, to, h).start()

        @pl.when((role < 2) & jnp.logical_not(outer))
        def _():
            to_inner(role, to, h).wait_recv()
            to_peer[slot] = (
                summed + merging[role * PARTS + h].astype(jnp.float32)
            ).astype(jnp.bfloat16)
            to_place(role, to, h).start()

        @pl.when(role == 2)
        def _():
            to_peer[slot] = summed.astype(jnp.bfloat16)
            to_pair(h).start()

        @pl.when(role == 3)
        def _():
            final[h] = summed

        return carry

    lax.fori_loop(0, places * PARTS, compute, 0)

    for h in range(PARTS):
        to_pair(h).wait_recv()
        total = final[h] + from_peer[PARTS + h].astype(jnp.float32)
        to_place(0, z, h).wait_recv()
        out_ref[h * part_rows : (h + 1) * part_rows, :] = (
            total + from_peer[h].astype(jnp.float32)
        ).astype(out_ref.dtype)

    inward.drain()
    outward.drain()

    for p in range(PIECES):

        @pl.when(z < places - 1)
        def _():
            right(0, p).wait_send()

        @pl.when(z > 0)
        def _():
            left(0, p).wait_send()

        share(0, z, c, p).wait_send()
        for k in range(1, places):

            @pl.when(z >= k)
            def _():
                @pl.when(z < places - 1)
                def _():
                    right(k, p).wait_send()

                share(k, z - k, c, p).wait_send()

            @pl.when(z + k < places)
            def _():
                @pl.when(z > 0)
                def _():
                    left(k, p).wait_send()

                share(places - 1 + k, z + k, c, p).wait_send()

    for step in range(places * PARTS):
        to_sibling(step).wait_send()
    for h in range(PARTS):
        for role, to in ((0, far), (1, near)):

            @pl.when(outer)
            def _():
                to_inner(role, to, h).wait_send()

            @pl.when(jnp.logical_not(outer))
            def _():
                to_place(role, to, h).wait_send()

        to_pair(h).wait_send()


def fused(
    tokens,
    norm_gain,
    pool_input,
    query_weight,
    key_weight,
    value_weight,
    pool_map,
    pool_scale,
    head_gain,
    diff_lambda,
    out_pool,
    out_heads,
):
    places = lax.axis_size("sp")
    groups = lax.axis_size("fs")
    row_count, model = tokens.shape[1], tokens.shape[2]
    length = places * row_count
    half = HEAD_DIM // 2
    freqs = 1.0 / THETA ** (jnp.arange(half, dtype=jnp.float32) * 2.0 / HEAD_DIM)
    freqs = jnp.concatenate([freqs, freqs])[None, :]
    group_count = pool_map.shape[0]
    half_out = model // 2
    vmem = pl.BlockSpec(memory_space=pltpu.VMEM)
    smem = pl.BlockSpec(memory_space=pltpu.SMEM)
    dma = pltpu.SemaphoreType.DMA
    low = jnp.bfloat16

    def gather_sems(count):
        return [
            dma((count,)),
            dma((places, count)),
            dma((places, count)),
            dma((2, 2 * places)),
            dma((2, 2 * places)),
            dma((2, places)),
            dma((2, places)),
        ]

    out = pl.pallas_call(
        lambda *refs: fused_kernel(places, groups, *refs),
        out_shape=jax.ShapeDtypeStruct((row_count, half_out), low),
        in_specs=[vmem] * 10 + [smem] + [vmem] * 2,
        out_specs=vmem,
        scratch_shapes=[
            pltpu.VMEM((row_count // 2, model), low),
            pltpu.VMEM((length, HEAD_DIM), jnp.float32),
            pltpu.VMEM((length, HEAD_DIM), jnp.float32),
            pltpu.VMEM((length, model), low),
            pltpu.VMEM((4, model, GROUP_DIM), low),
            pltpu.VMEM((2, GROUP_DIM, model), low),
            pltpu.VMEM((length, GROUP_DIM), low),
            pltpu.VMEM((length, GROUP_DIM), low),
            pltpu.VMEM((length, GROUP_DIM), low),
            pltpu.VMEM((length + 16, GROUP_DIM), low),
            pltpu.VMEM((places * PARTS, row_count // PARTS, half_out), low),
            pltpu.VMEM((places * PARTS, row_count // PARTS, half_out), low),
            pltpu.VMEM((places * PARTS, row_count // PARTS, half_out), low),
            pltpu.VMEM((2 * PARTS, row_count // PARTS, half_out), low),
            pltpu.VMEM((2 * PARTS, row_count // PARTS, half_out), low),
            pltpu.VMEM((PARTS, row_count // PARTS, half_out), jnp.float32),
            dma,
            *gather_sems(4),
            *gather_sems(2),
            dma((places, PIECES)),
            dma((places + 1, PIECES)),
            dma((places, PIECES)),
            dma((places + 1, PIECES)),
            dma((2 * places, PIECES)),
            dma((2 * places, PIECES)),
            dma((places * PARTS,)),
            dma((places * PARTS,)),
            dma((3 * PARTS,)),
            dma((2 * PARTS,)),
            dma((2 * PARTS,)),
            dma((2 * PARTS,)),
        ],
        compiler_params=pltpu.CompilerParams(
            collective_id=0, has_side_effects=True, vmem_limit_bytes=56 * 1024 * 1024
        ),
    )(
        tokens[0],
        norm_gain.reshape(1, model),
        freqs,
        pool_input,
        query_weight,
        key_weight,
        value_weight,
        pool_map,
        pool_scale.reshape(group_count, 1, GROUP_DIM),
        head_gain.reshape(1, 2 * HEAD_DIM),
        diff_lambda,
        out_pool,
        out_heads,
    )
    return out[None]


def solution(mesh):
    placed = (
        P("fs", "sp", None),
        P(),
        P(("sp", "fs"), "tp"),
        P(("sp", "fs"), "tp"),
        P(("sp", "fs"), "tp"),
        P(("sp", "fs"), "tp"),
        P("tp", None, None),
        P("tp"),
        P(),
        P(),
        P("tp", ("sp", "fs")),
        P("tp", ("sp", "fs")),
    )
    shape = dict(mesh.shape)

    def body(tokens, *rest):
        head_count = rest[3].shape[1] // (2 * HEAD_DIM)
        group_count = rest[5].shape[0]
        fits = (
            shape["fs"] == 4
            and shape["tp"] == 2
            and shape["sp"] == head_count == group_count == 4
            and tokens.shape[0] == 1
        )
        return (fused if fits else local)(tokens, *rest)

    return jax.shard_map(
        body, mesh=mesh, in_specs=placed, out_specs=P("fs", "sp", "tp"), check_vma=False
    )
```

profile of v0, /device:TPU:10, one launch (start us, length us, event | category | flops | bytes accessed | tf_op | source)
XLA Modules:
  0.0 126.4 jit_solution(15792883224216550993)
XLA Ops:
  0.0 0.6 maximum_bitcast_fusion.refs_2_
  0.6 123.9 %shard_map.118 = bf16[256,1024]{1,0:T(8,128)(2,1)} custom-call(bf16[256,2048]{1,0:T(8,128)(2,1)} %bitcast.8, f32[1,2048]{1,0:T(1,128)} %bitcast.9, f32[1,128]{1,0:T(1,128)} %maximum_bitcast_fusion.refs_2_, bf16[128,1024]{1,0:T(8,128)(2,1)} %refs_3_.1, bf16[128,1024]{1,0:T(8,128)(2,1)} %refs_4_.1, bf16[128,1024]{1,0:T(8,128)(2,1)} %refs_5_.1, ...), custom_call_target="tpu_custom_call" | custom-call | tf_op jit(solution)/shard_map/pallas_call | solution.py:798
  124.6 1.9 %copy.14 = bf16[1,256,1024]{2,1,0:T(8,128)(2,1)} copy(bf16[1,256,1024]{2,1,0:T(8,128)(2,1)} %bitcast.7) | data formatting | bytes 1048576
  (1 shorter events, 0.0 us)
where the time goes:
time: 127 us; the launch traced here: 126 us
  Pallas kernels  124 us (98%)
  local copies, waits for them, and re-layouts  1.87 us (1%)
    pallas_call x1, Pallas kernels, fused(): pl.pallas_call(lambda *refs: fused_kernel(places, groups, *refs), out_sha...  124 us

commit v1 on v0

--- a/solution.py
+++ b/solution.py
@@ -2,6 +2,7 @@
 
 import jax
 import jax.numpy as jnp
+import numpy as np
 from jax import lax
 from jax.experimental import pallas as pl
 from jax.experimental.pallas import tpu as pltpu
@@ -192,6 +193,22 @@
 PIECES = 4
 PARTS = 2
 
+PROJECTED = ((0, 1, 2, 3), (1, 0, 2, 3), (2, 3, 0, 1), (3, 2, 0, 1))
+FINISHED = ((1, 3, 2, 0), (0, 3, 2, 1), (0, 1, 3, 2), (0, 1, 2, 3))
+ARRIVALS = ((0, 1, 2, 3), (1, 0, 2, 3), (2, 3, 1, 0), (3, 2, 1, 0))
+SENDS = ((0, 1, 2, 3), (1, 3, 2, 0), (2, 0, 1, 3), (3, 2, 1, 0))
+SLOTS = tuple(
+    tuple(ARRIVALS[to].index(place) for to in SENDS[place]) for place in range(len(SENDS))
+)
+
+
+def pick(row, z):
+    value = jnp.int32(row[0])
+    for place in range(1, len(row)):
+        value = jnp.where(z == place, row[place], value)
+    return value
+
+
 def fused_kernel(
     places,
     groups,
@@ -209,7 +226,8 @@
     out_pool_ref,
     out_heads_ref,
     out_ref,
-    normed_ref,
+    own_tokens,
+    own_map,
     cos_ref,
     sin_ref,
     rows_all,
@@ -219,8 +237,10 @@
     keys,
     values,
     pools,
+    mine,
     to_mate,
     from_mate,
+    kept,
     to_peer,
     from_peer,
     merging,
@@ -268,13 +288,20 @@
     width = GROUP_DIM
     out_width = out_pool_ref.shape[1]
     half_out = out_ref.shape[1]
+    length = places * row_count
+
+    send_to = [pick([row[d] for row in SENDS], z) for d in range(places)]
+    send_slot = [pick([row[d] for row in SLOTS], z) for d in range(places)]
+    source = [pick([row[d] for row in ARRIVALS], z) for d in range(places)]
+
+    def block(index, size):
+        return pl.ds(pl.multiple_of(index * size, size), size)
 
     barrier = pltpu.get_barrier_semaphore()
     partners = [{"sp": lax.rem(z + d, places)} for d in range(1, places)]
     partners += [{"fs": fx}, {"fs": fy}, {"tp": mate}]
     for partner in partners:
         pl.semaphore_signal(barrier, inc=1, device_id=partner, device_id_type=MESH)
-    pl.semaphore_wait(barrier, len(partners))
 
     def remote(source, target, send, recv, device):
         return pltpu.make_async_remote_copy(
@@ -285,9 +312,6 @@
             device_id=device,
             device_id_type=MESH,
         )
-
-    def block(index, size):
-        return pl.ds(pl.multiple_of(index * size, size), size)
 
     class Gather:
         def __init__(self, sources, cut, view, group):
@@ -311,28 +335,24 @@
             )
 
         def across(self, d, m):
-            to = lax.rem(z + d, places)
+            to, slot = send_to[d], send_slot[d]
             return remote(
                 self.cut(self.sources[m], to),
                 self.view(z, f, m, 1).at[0],
                 self.z_send.at[d, m],
-                self.z_recv.at[d, m],
+                self.z_recv.at[slot, m],
                 {"sp": to},
             )
 
         def arrive(self, d, m):
-            view = self.view(lax.rem(z + places - d, places), f, m, 1).at[0]
+            view = self.view(source[d], f, m, 1).at[0]
             return remote(
-                view,
-                view,
-                self.z_send.at[d, m],
-                self.z_recv.at[d, m],
-                {"sp": lax.rem(z + places - d, places)},
+                view, view, self.z_send.at[d, m], self.z_recv.at[d, m], {"sp": source[d]}
             )
 
         def near(self, d, side, column, half):
             start, size = (self.low, self.high)[half]
-            view = self.view(lax.rem(z + places - d, places), column, start, size)
+            view = self.view(source[d], column, start, size)
             return remote(
                 view,
                 view,
@@ -343,7 +363,7 @@
 
         def forward(self, d, side, column):
             start, size = (self.high, self.low)[side]
-            view = self.view(lax.rem(z + places - d, places), column, start, size)
+            view = self.view(source[d], column, start, size)
             return remote(
                 view,
                 view,
@@ -352,12 +372,13 @@
                 {"fs": (fx, fy)[side]},
             )
 
-        def start(self):
+        def start_own(self):
             for m in range(self.count):
                 self.own(m).start()
-            for d in range(1, places):
-                for m in range(self.count):
-                    self.across(d, m).start()
+
+        def start(self, d):
+            for m in range(self.count):
+                self.across(d, m).start()
 
         def first(self, d):
             for m in range(self.count):
@@ -408,83 +429,84 @@
 
     piece_rows = half_rows // PIECES
 
-    def chunk(zz, side, p):
-        return rows_all.at[block((2 * zz + side) * PIECES + p, piece_rows), :]
-
-    def right(k, p):
-        view = chunk(z - k, c, p)
-        return remote(view, view, right_send.at[k, p], right_recv.at[k + 1, p], {"sp": z + 1})
-
-    def from_left(k, p):
-        view = chunk(z - k, c, p)
-        return remote(view, view, right_send.at[k, p], right_recv.at[k, p], {"sp": z - 1})
-
-    def left(k, p):
-        view = chunk(z + k, c, p)
-        return remote(view, view, left_send.at[k, p], left_recv.at[k + 1, p], {"sp": z - 1})
-
-    def from_right(k, p):
-        view = chunk(z + k, c, p)
-        return remote(view, view, left_send.at[k, p], left_recv.at[k, p], {"sp": z + 1})
-
-    def share(slot, zz, side, p):
-        view = chunk(zz, side, p)
-        return remote(view, view, mate_send.at[slot, p], mate_recv.at[slot, p], {"tp": mate})
-
-    own_rows = pltpu.make_async_copy(
-        normed_ref, rows_all.at[block(2 * z + c, half_rows), :], own_sem
-    )
-    inward.start()
-    outward.start()
-    floated = tokens_ref[pl.ds(pl.multiple_of(c * half_rows, 16), half_rows), :].astype(
-        jnp.float32
-    )
-    normed_ref[...] = (
+    def chunk(b, side, p):
+        return rows_all.at[block((2 * b + side) * PIECES + p, piece_rows), :]
+
+    def right(b, p, step=1):
+        view = chunk(b, c, p)
+        return remote(view, view, right_send.at[b, p], right_recv.at[b, p], {"sp": z + step})
+
+    def left(b, p, step=-1):
+        view = chunk(b, c, p)
+        return remote(view, view, left_send.at[b, p], left_recv.at[b, p], {"sp": z + step})
+
+    def share(b, side, p):
+        view = chunk(b, side, p)
+        return remote(view, view, mate_send.at[b, p], mate_recv.at[b, p], {"tp": mate})
+
+    def each_place(act):
+        for place in range(places):
+            pl.when(z == place)(lambda place=place: act(place))
+
+    def own_sends(turn):
+        def act(place):
+            for p in range(PIECES):
+                if (place, turn) in ((places - 1, 0), (1, 1), (2, 2)):
+                    left(place, p).start()
+                if (place, turn) in ((0, 0), (2, 1)):
+                    right(place, p).start()
+                if turn == 0:
+                    share(place, c, p).start()
+
+        each_place(act)
+
+    def take(place, b, p):
+        if b < place:
+            right(b, p, -1).wait_recv()
+            if place < places - 1:
+                right(b, p).start()
+        else:
+            left(b, p, 1).wait_recv()
+            if place > 0:
+                left(b, p).start()
+        share(b, c, p).start()
+
+    def taken(blocks):
+        def act(place):
+            b = blocks[place]
+            if b is None:
+                return
+            for p in range(PIECES):
+                take(place, b, p)
+            if place == 1 and b == 0:
+                for p in range(PIECES):
+                    right(place, p).start()
+
+        each_place(act)
+
+    tokens_in = pltpu.make_async_copy(
+        tokens_ref.at[block(c, half_rows), :], own_tokens, own_sem.at[0]
+    )
+    map_in = pltpu.make_async_copy(map_ref.at[z], own_map, own_sem.at[1])
+    tokens_in.start()
+    inward.start_own()
+    outward.start_own()
+    map_in.start()
+    pl.semaphore_wait(barrier, len(partners))
+    for d in range(1, places):
+        inward.start(d)
+    tokens_in.wait()
+    floated = own_tokens[...].astype(jnp.float32)
+    rows_all[block(2 * z + c, half_rows), :] = (
         floated
         * lax.rsqrt(jnp.mean(floated * floated, -1, keepdims=True) + NORM_EPS)
         * norm_gain_ref[...]
     ).astype(jnp.bfloat16)
-    own_rows.start()
-    own_rows.wait()
-
-    @pl.when(z < places - 1)
-    def _():
-        for p in range(PIECES):
-            right(0, p).start()
-
-    @pl.when(z > 0)
-    def _():
-        for p in range(PIECES):
-            left(0, p).start()
-
-    for p in range(PIECES):
-        share(0, z, c, p).start()
-
-    def tokens_step(k):
-        for p in range(PIECES):
-
-            @pl.when(z >= k)
-            def _():
-                from_left(k, p).wait_recv()
-
-                @pl.when(z < places - 1)
-                def _():
-                    right(k, p).start()
-
-                share(k, z - k, c, p).start()
-
-            @pl.when(z + k < places)
-            def _():
-                from_right(k, p).wait_recv()
-
-                @pl.when(z > 0)
-                def _():
-                    left(k, p).start()
-
-                share(places - 1 + k, z + k, c, p).start()
-
+    inward.first(0)
     pools[0:16, :] = jnp.zeros((16, width), jnp.bfloat16)
-    inward.first(0)
+    keys[...] = jnp.zeros_like(keys)
+    values[...] = jnp.zeros_like(values)
+    own_sends(0)
 
     def table(index, carry):
         rows = block(index, row_count)
@@ -500,34 +522,6 @@
         return carry
 
     lax.fori_loop(0, places, table, 0)
-    for d in range(1, places):
-        inward.first(d)
-        inward.second(d - 1)
-    outward.first(0)
-    inward.second(places - 1)
-    for d in range(1, places):
-        outward.first(d)
-        if d > 1:
-            outward.second(d - 2)
-    tokens_step(1)
-    for d in (places - 2, places - 1):
-        outward.second(d)
-    for k in range(2, places):
-        tokens_step(k)
-    for d in range(places):
-        inward.third(d)
-
-    for p in range(PIECES):
-        share(0, z, mate, p).wait_recv()
-        for k in range(1, places):
-
-            @pl.when(z >= k)
-            def _():
-                share(k, z - k, mate, p).wait_recv()
-
-            @pl.when(z + k < places)
-            def _():
-                share(places - 1 + k, z + k, mate, p).wait_recv()
 
     def turned(raw, cosine, sine):
         floated = raw.astype(jnp.float32)
@@ -535,7 +529,12 @@
             jnp.bfloat16
         )
 
-    def project(index, carry):
+    projected = [pick([row[i] for row in PROJECTED], z) for i in range(places)]
+    finished = [pick([row[i] for row in FINISHED], z) for i in range(places)]
+
+    def project(index):
+        for p in range(PIECES):
+            share(index, mate, p).wait_recv()
         rows = block(index, row_count)
         normed = rows_all[rows, :]
         cosine = cos_ref[rows, :]
@@ -556,9 +555,39 @@
             part = slice(m * HEAD_DIM, (m + 1) * HEAD_DIM)
             keys[rows, part] = turned(raw[:, part], cosine, sine)
         values[rows, :] = product(3)
+
+    def project_early(i, carry):
+        project(jnp.where(i == 0, projected[0], projected[1]))
         return carry
 
-    lax.fori_loop(0, places, project, 0)
+    inward.first(1)
+    own_sends(1)
+    inward.second(0)
+    inward.first(2)
+    for d in range(1, places):
+        outward.start(d)
+    own_sends(2)
+    inward.second(1)
+    inward.first(3)
+    inward.second(2)
+    taken((1, 0, 3, 2))
+    inward.second(3)
+    outward.first(0)
+    outward.first(1)
+    taken((None, 2, None, None))
+    for d in range(places):
+        inward.third(d)
+    outward.first(2)
+    outward.first(3)
+    lax.fori_loop(0, 2, project_early, 0)
+    outward.second(0)
+    taken((2, None, 0, 0))
+    outward.second(1)
+    outward.second(2)
+    project(projected[2])
+    outward.second(3)
+    taken((None, 3, 1, None))
+    map_in.wait()
     for d in range(places):
         outward.third(d)
 
@@ -567,7 +596,6 @@
         level == 0, 2, jnp.where(level == 1, 4, jnp.where(level == 2, 8, 16))
     )
     head_lambda = lambda_ref[c * map_ref.shape[0] + z]
-    length = places * row_count
 
     part_rows = row_count // PARTS
 
@@ -582,23 +610,24 @@
 
     outer = (z == 0) | (z == places - 1)
     pair = z + 1 - 2 * lax.rem(z, 2)
-    far = jnp.where(z < 2, places - 1, 0)
-    near = jnp.where(z < 2, 2, 1)
-
-    def to_inner(role, to, h):
+
+    def crossing(to, h):
+        return lax.rem(to, 2) * PARTS + h
+
+    def to_inner(to, h):
         return remote(
             to_peer.at[to * PARTS + h],
-            merging.at[role * PARTS + h],
-            merge_send.at[role * PARTS + h],
-            merge_recv.at[role * PARTS + h],
+            merging.at[crossing(to, h)],
+            merge_send.at[crossing(to, h)],
+            merge_recv.at[crossing(to, h)],
             {"sp": pair},
         )
 
-    def to_place(role, to, h):
+    def to_place(to, h):
         return remote(
             to_peer.at[to * PARTS + h],
             from_peer.at[h],
-            peer_send.at[role * PARTS + h],
+            peer_send.at[crossing(to, h)],
             peer_recv.at[h],
             {"sp": to},
         )
@@ -612,11 +641,15 @@
             {"sp": pair},
         )
 
-    def compute(step, carry):
+    def step_place(step):
         turn = step // PARTS
-        h = lax.rem(step, PARTS)
-        role = jnp.where((turn == 3) | outer, turn, lax.rem(turn + 2, 3))
-        to = jnp.where(role == 0, far, jnp.where(role == 1, near, jnp.where(role == 2, pair, z)))
+        to = finished[places - 1]
+        for i in range(places - 1):
+            to = jnp.where(turn == i, finished[i], to)
+        return to, lax.rem(step, PARTS)
+
+    def compute(step):
+        to, h = step_place(step)
         slot = to * PARTS + h
         rows = block(slot, part_rows)
         query_pos = slot * part_rows + lax.broadcasted_iota(jnp.int32, (part_rows, length), 0)
@@ -659,7 +692,7 @@
         counts = jnp.minimum(places_of + 1, window).astype(jnp.float32)
         mixed = (picked[16:] / counts - extended[16:]).astype(jnp.bfloat16)
         pooled = (
-            jnp.dot(mixed, map_ref[z], preferred_element_type=jnp.float32) * scale_ref[z]
+            jnp.dot(mixed, own_map[...], preferred_element_type=jnp.float32) * scale_ref[z]
         ).astype(jnp.bfloat16)
 
         def partial_of(side):
@@ -670,40 +703,82 @@
 
         to_mate[step] = partial_of(mate).astype(jnp.bfloat16)
         to_sibling(step).start()
-        mine = partial_of(c)
+        mine[lax.rem(step, 2)] = partial_of(c)
+
+    def finish(step):
+        to, h = step_place(step)
+        slot = to * PARTS + h
+        crosses = to // 2 != z // 2
         to_sibling(step).wait_recv()
-        summed = mine + from_mate[step].astype(jnp.float32)
-
-        @pl.when((role < 2) & outer)
+        summed = mine[lax.rem(step, 2)] + from_mate[step].astype(jnp.float32)
+
+        @pl.when(to == z)
         def _():
-            to_peer[slot] = summed.astype(jnp.bfloat16)
-            to_inner(role, to, h).start()
-
-        @pl.when((role < 2) & jnp.logical_not(outer))
-        def _():
-            to_inner(role, to, h).wait_recv()
-            to_peer[slot] = (
-                summed + merging[role * PARTS + h].astype(jnp.float32)
-            ).astype(jnp.bfloat16)
-            to_place(role, to, h).start()
-
-        @pl.when(role == 2)
+            final[h] = summed
+
+        @pl.when(to == pair)
         def _():
             to_peer[slot] = summed.astype(jnp.bfloat16)
             to_pair(h).start()
 
-        @pl.when(role == 3)
+        @pl.when(crosses & outer)
         def _():
-            final[h] = summed
+            to_peer[slot] = summed.astype(jnp.bfloat16)
+            to_inner(to, h).start()
+
+        @pl.when(crosses & jnp.logical_not(outer))
+        def _():
+            kept[crossing(to, h)] = summed
+
+    def merge(turn):
+        place = turn // PARTS
+        to = jnp.where(z < places // 2, places - 1 - place, place)
+        h = lax.rem(turn, PARTS)
+        to_inner(to, h).wait_recv()
+        to_peer[to * PARTS + h] = (
+            kept[crossing(to, h)] + merging[crossing(to, h)].astype(jnp.float32)
+        ).astype(jnp.bfloat16)
+        to_place(to, h).start()
+
+    upper_inner = z == places // 2
+
+    def body(step, carry):
+        @pl.when(step == PARTS)
+        def _():
+            taken((3, None, None, 1))
+            project(projected[3])
+
+        compute(step)
+
+        @pl.when(step > 0)
+        def _():
+            finish(step - 1)
+
+        @pl.when(upper_inner & (step > 2) & (lax.rem(step, 2) == 1))
+        def _():
+            merge((step - 3) // 2)
 
         return carry
 
-    lax.fori_loop(0, places * PARTS, compute, 0)
+    lax.fori_loop(0, places * PARTS, body, 0)
+    finish(places * PARTS - 1)
+
+    def merge_more(turn, carry):
+        merge(turn)
+        return carry
+
+    @pl.when(z == places // 2 - 1)
+    def _():
+        lax.fori_loop(0, 2 * PARTS, merge_more, 0)
+
+    @pl.when(upper_inner)
+    def _():
+        merge(2 * PARTS - 1)
 
     for h in range(PARTS):
         to_pair(h).wait_recv()
         total = final[h] + from_peer[PARTS + h].astype(jnp.float32)
-        to_place(0, z, h).wait_recv()
+        to_place(z, h).wait_recv()
         out_ref[h * part_rows : (h + 1) * part_rows, :] = (
             total + from_peer[h].astype(jnp.float32)
         ).astype(out_ref.dtype)
@@ -711,49 +786,26 @@
     inward.drain()
     outward.drain()
 
-    for p in range(PIECES):
-
-        @pl.when(z < places - 1)
-        def _():
-            right(0, p).wait_send()
-
-        @pl.when(z > 0)
-        def _():
-            left(0, p).wait_send()
-
-        share(0, z, c, p).wait_send()
-        for k in range(1, places):
-
-            @pl.when(z >= k)
-            def _():
-                @pl.when(z < places - 1)
-                def _():
-                    right(k, p).wait_send()
-
-                share(k, z - k, c, p).wait_send()
-
-            @pl.when(z + k < places)
-            def _():
-                @pl.when(z > 0)
-                def _():
-                    left(k, p).wait_send()
-
-                share(places - 1 + k, z + k, c, p).wait_send()
-
+    def drain(place):
+        for b in range(places):
+            for p in range(PIECES):
+                if b <= place < places - 1:
+                    right(b, p).wait_send()
+                if b >= place > 0:
+                    left(b, p).wait_send()
+                share(b, c, p).wait_send()
+        for h in range(PARTS):
+            to_pair(h).wait_send()
+            for to in range(places):
+                if to // 2 != place // 2:
+                    if place in (0, places - 1):
+                        to_inner(to, h).wait_send()
+                    else:
+                        to_place(to, h).wait_send()
+
+    each_place(drain)
     for step in range(places * PARTS):
         to_sibling(step).wait_send()
-    for h in range(PARTS):
-        for role, to in ((0, far), (1, near)):
-
-            @pl.when(outer)
-            def _():
-                to_inner(role, to, h).wait_send()
-
-            @pl.when(jnp.logical_not(outer))
-            def _():
-                to_place(role, to, h).wait_send()
-
-        to_pair(h).wait_send()
 
 
 def fused(
@@ -775,12 +827,15 @@
     row_count, model = tokens.shape[1], tokens.shape[2]
     length = places * row_count
     half = HEAD_DIM // 2
-    freqs = 1.0 / THETA ** (jnp.arange(half, dtype=jnp.float32) * 2.0 / HEAD_DIM)
-    freqs = jnp.concatenate([freqs, freqs])[None, :]
+    freqs = np.float32(1.0) / np.float32(THETA) ** (
+        np.arange(half, dtype=np.float32) * np.float32(2.0) / np.float32(HEAD_DIM)
+    )
+    freqs = jnp.asarray(np.concatenate([freqs, freqs])[None, :], jnp.float32)
     group_count = pool_map.shape[0]
     half_out = model // 2
     vmem = pl.BlockSpec(memory_space=pltpu.VMEM)
     smem = pl.BlockSpec(memory_space=pltpu.SMEM)
+    hbm = pl.BlockSpec(memory_space=pl.ANY)
     dma = pltpu.SemaphoreType.DMA
     low = jnp.bfloat16
 
@@ -798,10 +853,11 @@
     out = pl.pallas_call(
         lambda *refs: fused_kernel(places, groups, *refs),
         out_shape=jax.ShapeDtypeStruct((row_count, half_out), low),
-        in_specs=[vmem] * 10 + [smem] + [vmem] * 2,
+        in_specs=[hbm, vmem, vmem] + [hbm] * 5 + [vmem] * 2 + [smem] + [hbm] * 2,
         out_specs=vmem,
         scratch_shapes=[
             pltpu.VMEM((row_count // 2, model), low),
+            pltpu.VMEM((GROUP_DIM, GROUP_DIM), low),
             pltpu.VMEM((length, HEAD_DIM), jnp.float32),
             pltpu.VMEM((length, HEAD_DIM), jnp.float32),
             pltpu.VMEM((length, model), low),
@@ -811,21 +867,23 @@
             pltpu.VMEM((length, GROUP_DIM), low),
             pltpu.VMEM((length, GROUP_DIM), low),
             pltpu.VMEM((length + 16, GROUP_DIM), low),
+            pltpu.VMEM((2, row_count // PARTS, half_out), jnp.float32),
             pltpu.VMEM((places * PARTS, row_count // PARTS, half_out), low),
             pltpu.VMEM((places * PARTS, row_count // PARTS, half_out), low),
+            pltpu.VMEM((2 * PARTS, row_count // PARTS, half_out), jnp.float32),
             pltpu.VMEM((places * PARTS, row_count // PARTS, half_out), low),
             pltpu.VMEM((2 * PARTS, row_count // PARTS, half_out), low),
             pltpu.VMEM((2 * PARTS, row_count // PARTS, half_out), low),
             pltpu.VMEM((PARTS, row_count // PARTS, half_out), jnp.float32),
-            dma,
+            dma((2,)),
             *gather_sems(4),
             *gather_sems(2),
             dma((places, PIECES)),
-            dma((places + 1, PIECES)),
             dma((places, PIECES)),
-            dma((places + 1, PIECES)),
-            dma((2 * places, PIECES)),
-            dma((2 * places, PIECES)),
+            dma((places, PIECES)),
+            dma((places, PIECES)),
+            dma((places, PIECES)),
+            dma((places, PIECES)),
             dma((places * PARTS,)),
             dma((places * PARTS,)),
             dma((3 * PARTS,)),

time: 127 us -> 117 us (0.921)
  the two profiles are of different devices: /device:TPU:10 before, /device:TPU:16 now
where the time goes in v1:
time: 117 us
  Pallas kernels  115 us (98%)
  local copies, waits for them, and re-layouts  1.87 us (2%)
    pallas_call x1, Pallas kernels, fused(): pl.pallas_call(lambda *refs: fused_kernel(places, groups, *refs), out_sha...  115 us

profile of v1, /device:TPU:16, one launch (start us, length us, event | category | flops | bytes accessed | tf_op | source)
XLA Modules:
  0.0 116.6 jit_solution(10355418743483961518)
XLA Ops:
  0.0 114.8 %shard_map.127 = bf16[256,1024]{1,0:T(8,128)(2,1)} custom-call(bf16[256,2048]{1,0:T(8,128)(2,1)} %bitcast.6, f32[1,2048]{1,0:T(1,128)} %bitcast.7, f32[1,128]{1,0:T(1,128)} %constant.2.clone.refs_2_, bf16[128,1024]{1,0:T(8,128)(2,1)} %refs_3_.1, bf16[128,1024]{1,0:T(8,128)(2,1)} %refs_4_.1, bf16[128,1024]{1,0:T(8,128)(2,1)} %refs_5_.1, ...), custom_call_target="tpu_custom_call" | custom-call | tf_op jit(solution)/shard_map/pallas_call | solution.py:853
  114.8 1.9 %copy.15 = bf16[1,256,1024]{2,1,0:T(8,128)(2,1)} copy(bf16[1,256,1024]{2,1,0:T(8,128)(2,1)} %bitcast.5) | data formatting | bytes 1048576

commit v2 on v1

--- a/solution.py
+++ b/solution.py
@@ -194,8 +194,14 @@
 PARTS = 2
 
 PROJECTED = ((0, 1, 2, 3), (1, 0, 2, 3), (2, 3, 0, 1), (3, 2, 0, 1))
-FINISHED = ((1, 3, 2, 0), (0, 3, 2, 1), (0, 1, 3, 2), (0, 1, 2, 3))
-ARRIVALS = ((0, 1, 2, 3), (1, 0, 2, 3), (2, 3, 1, 0), (3, 2, 1, 0))
+LATE = ((1, 3), (2, 4), (-1, 2), (-1, 2))
+FINISHED = (
+    (2, 4, 5, 6, 7, 3, 0, 1),
+    (2, 3, 4, 5, 6, 7, 0, 1),
+    (0, 1, 2, 3, 6, 7, 4, 5),
+    (0, 1, 2, 3, 4, 5, 6, 7),
+)
+ARRIVALS = ((0, 1, 2, 3), (1, 0, 3, 2), (2, 3, 0, 1), (3, 2, 1, 0))
 SENDS = ((0, 1, 2, 3), (1, 3, 2, 0), (2, 0, 1, 3), (3, 2, 1, 0))
 SLOTS = tuple(
     tuple(ARRIVALS[to].index(place) for to in SENDS[place]) for place in range(len(SENDS))
@@ -254,26 +260,20 @@
         in_z_recv,
         in_n_send,
         in_n_recv,
-        in_f_send,
-        in_f_recv,
+        in_rest,
         out_local,
         out_z_send,
         out_z_recv,
         out_n_send,
         out_n_recv,
-        out_f_send,
-        out_f_recv,
-        right_send,
-        right_recv,
-        left_send,
-        left_recv,
-        mate_send,
+        out_rest,
+        token_send,
+        token_recv,
         mate_recv,
         half_send,
         half_recv,
         peer_send,
         peer_recv,
-        merge_send,
         merge_recv,
     ) = sems
     z = lax.axis_index("sp")
@@ -314,8 +314,9 @@
         )
 
     class Gather:
-        def __init__(self, sources, cut, view, group):
+        def __init__(self, sources, cut, view, sent, received, group):
             self.sources, self.cut, self.view = sources, cut, view
+            self.sent, self.received = sent, received
             self.count = len(sources)
             (
                 self.local,
@@ -323,8 +324,7 @@
                 self.z_recv,
                 self.n_send,
                 self.n_recv,
-                self.f_send,
-                self.f_recv,
+                self.rest,
             ) = group
             self.low = (0, self.count // 2)
             self.high = (self.count // 2, self.count - self.count // 2)
@@ -339,25 +339,24 @@
             return remote(
                 self.cut(self.sources[m], to),
                 self.view(z, f, m, 1).at[0],
-                self.z_send.at[d, m],
-                self.z_recv.at[slot, m],
+                self.z_send.at[d],
+                self.z_recv.at[slot],
                 {"sp": to},
             )
 
-        def arrive(self, d, m):
-            view = self.view(source[d], f, m, 1).at[0]
-            return remote(
-                view, view, self.z_send.at[d, m], self.z_recv.at[d, m], {"sp": source[d]}
-            )
+        def arrive(self, d):
+            view = self.view(source[d], f, 0, self.count)
+            return remote(view, view, self.z_send.at[d], self.z_recv.at[d], {"sp": source[d]})
 
         def near(self, d, side, column, half):
             start, size = (self.low, self.high)[half]
             view = self.view(source[d], column, start, size)
+            early = half == side
             return remote(
                 view,
                 view,
-                self.n_send.at[side, 2 * d + half],
-                self.n_recv.at[side, 2 * d + half],
+                self.n_send.at[side],
+                self.n_recv.at[side, d] if early else self.rest.at[0],
                 {"fs": (fx, fy)[side]},
             )
 
@@ -365,11 +364,7 @@
             start, size = (self.high, self.low)[side]
             view = self.view(source[d], column, start, size)
             return remote(
-                view,
-                view,
-                self.f_send.at[side, d],
-                self.f_recv.at[side, d],
-                {"fs": (fx, fy)[side]},
+                view, view, self.n_send.at[side], self.rest.at[0], {"fs": (fx, fy)[side]}
             )
 
         def start_own(self):
@@ -381,11 +376,11 @@
                 self.across(d, m).start()
 
         def first(self, d):
-            for m in range(self.count):
-                if d == 0:
+            if d == 0:
+                for m in range(self.count):
                     self.own(m).wait()
-                else:
-                    self.arrive(d, m).wait_recv()
+            else:
+                self.arrive(d).wait_recv()
             for order in range(2):
                 for side in range(2):
                     self.near(d, side, f, side ^ order).start()
@@ -396,35 +391,35 @@
             self.near(d, 1, fy, 1).wait_recv()
             self.forward(d, 0, fy).start()
 
-        def third(self, d):
-            diagonal = lax.rem(fx + 2, groups)
+        def third(self):
+            remote(
+                self.received, self.received, self.n_send.at[0], self.rest.at[0], {"fs": fx}
+            ).wait_recv()
+
+        def drain(self):
+            for d in range(1, places):
+                self.arrive(d).wait_send()
             for side in range(2):
-                self.forward(d, side, diagonal).wait_recv()
-            self.near(d, 0, fx, 1).wait_recv()
-            self.near(d, 1, fy, 0).wait_recv()
-
-        def drain(self):
-            for d in range(places):
-                for m in range(self.count):
-                    if d > 0:
-                        self.across(d, m).wait_send()
-                for side in range(2):
-                    for half in range(2):
-                        self.near(d, side, f, half).wait_send()
-                self.forward(d, 1, fx).wait_send()
-                self.forward(d, 0, fy).wait_send()
-
+                remote(
+                    self.sent, self.sent, self.n_send.at[side], self.rest.at[0], {"fs": fx}
+                ).wait_send()
+
+    filled = places * groups
     inward = Gather(
         (pool_ref, query_ref, key_ref, value_ref),
         lambda ref, to: ref.at[:, block(to, width)],
         lambda zz, ff, m, n: weights.at[pl.ds(m, n), block(zz * groups + ff, depth), :],
-        (in_local, in_z_send, in_z_recv, in_n_send, in_n_recv, in_f_send, in_f_recv),
+        weights.at[:, pl.ds(0, filled * 3 // 8 * depth), :],
+        weights.at[:, pl.ds(0, filled // 2 * depth), :],
+        (in_local, in_z_send, in_z_recv, in_n_send, in_n_recv, in_rest),
     )
     outward = Gather(
         (out_pool_ref, out_heads_ref),
         lambda ref, to: ref.at[block(to, width), :],
         lambda zz, ff, m, n: outs.at[pl.ds(m, n), :, block(zz * groups + ff, out_width)],
-        (out_local, out_z_send, out_z_recv, out_n_send, out_n_recv, out_f_send, out_f_recv),
+        outs.at[:, :, pl.ds(0, filled * 3 // 8 * out_width)],
+        outs.at[:, :, pl.ds(0, filled // 2 * out_width)],
+        (out_local, out_z_send, out_z_recv, out_n_send, out_n_recv, out_rest),
     )
 
     piece_rows = half_rows // PIECES
@@ -434,55 +429,117 @@
 
     def right(b, p, step=1):
         view = chunk(b, c, p)
-        return remote(view, view, right_send.at[b, p], right_recv.at[b, p], {"sp": z + step})
+        return remote(view, view, token_send.at[0], token_recv.at[b, p], {"sp": z + step})
 
     def left(b, p, step=-1):
         view = chunk(b, c, p)
-        return remote(view, view, left_send.at[b, p], left_recv.at[b, p], {"sp": z + step})
+        return remote(view, view, token_send.at[1], token_recv.at[b, p], {"sp": z + step})
 
     def share(b, side, p):
         view = chunk(b, side, p)
-        return remote(view, view, mate_send.at[b, p], mate_recv.at[b, p], {"tp": mate})
+        return remote(view, view, token_send.at[2], mate_recv.at[b], {"tp": mate})
+
+    def sent_tokens(kind, blocks):
+        view = rows_all.at[pl.ds(0, blocks * half_rows), :]
+        return remote(view, view, token_send.at[kind], mate_recv.at[0], {"tp": mate})
 
     def each_place(act):
         for place in range(places):
             pl.when(z == place)(lambda place=place: act(place))
 
-    def own_sends(turn):
-        def act(place):
-            for p in range(PIECES):
-                if (place, turn) in ((places - 1, 0), (1, 1), (2, 2)):
-                    left(place, p).start()
-                if (place, turn) in ((0, 0), (2, 1)):
-                    right(place, p).start()
-                if turn == 0:
-                    share(place, c, p).start()
-
-        each_place(act)
-
-    def take(place, b, p):
-        if b < place:
-            right(b, p, -1).wait_recv()
-            if place < places - 1:
-                right(b, p).start()
+    def send_right(place):
+        for p in range(PIECES):
+            right(place, p).start()
+
+    def send_left(place):
+        for p in range(PIECES):
+            left(place, p).start()
+
+    def take(place, b, pieces=range(PIECES)):
+        for p in pieces:
+            if b < place:
+                right(b, p, -1).wait_recv()
+                if place < places - 1:
+                    right(b, p).start()
+            else:
+                left(b, p, 1).wait_recv()
+                if place > 0:
+                    left(b, p).start()
+            share(b, c, p).start()
+
+    first_half, second_half = range(PIECES // 2), range(PIECES // 2, PIECES)
+
+    def prepare(place):
+        for d in range(1, places):
+            inward.start(d)
+        for d in range(1, places) if place in (1, 2) else (1,):
+            outward.start(d)
+
+    def begin(place):
+        if place == 0:
+            send_right(place)
+        if place == places - 1:
+            send_left(place)
+        if place in (0, places - 1):
+            for d in range(2, places):
+                outward.start(d)
+        for p in range(PIECES):
+            share(place, c, p).start()
+
+    def gather(place):
+        taken = (1, 0, 3, 2)[place]
+        inward.second(0)
+        outward.second(0)
+        inward.first(1)
+        inward.first(2)
+        if place in (1, 2):
+            if place == 1:
+                send_left(place)
+            else:
+                send_right(place)
+                send_left(place)
+            inward.second(1)
+            outward.first(1)
+            inward.second(2)
+            take(place, taken, first_half)
+            inward.first(3)
+            outward.first(3)
+            take(place, taken, second_half)
+            if place == 1:
+                send_right(place)
+            outward.second(1)
+            inward.second(3)
+            outward.first(2)
+            take(place, (None, 2, 0, None)[place], first_half)
         else:
-            left(b, p, 1).wait_recv()
-            if place > 0:
-                left(b, p).start()
-        share(b, c, p).start()
-
-    def taken(blocks):
-        def act(place):
-            b = blocks[place]
-            if b is None:
-                return
-            for p in range(PIECES):
-                take(place, b, p)
-            if place == 1 and b == 0:
-                for p in range(PIECES):
-                    right(place, p).start()
-
-        each_place(act)
+            inward.second(1)
+            inward.first(3)
+            outward.first(1)
+            inward.second(2)
+            outward.first(2)
+            inward.second(3)
+            outward.second(1)
+            take(place, taken)
+            outward.first(3)
+        inward.third()
+
+    def relay(place):
+        if place in (1, 2):
+            take(place, (None, 2, 0, None)[place], second_half)
+            outward.second(3)
+            outward.second(2)
+        else:
+            outward.second(2)
+            outward.second(3)
+        if place == 3:
+            take(place, 0)
+
+    def finish_gather(place):
+        if place in (1, 2):
+            take(place, (None, 3, 1, None)[place], first_half)
+        outward.third()
+        if place in (1, 2):
+            take(place, (None, 3, 1, None)[place], second_half)
 
     tokens_in = pltpu.make_async_copy(
         tokens_ref.at[block(c, half_rows), :], own_tokens, own_sem.at[0]
@@ -493,8 +550,7 @@
     outward.start_own()
     map_in.start()
     pl.semaphore_wait(barrier, len(partners))
-    for d in range(1, places):
-        inward.start(d)
+    each_place(prepare)
     tokens_in.wait()
     floated = own_tokens[...].astype(jnp.float32)
     rows_all[block(2 * z + c, half_rows), :] = (
@@ -503,10 +559,11 @@
         * norm_gain_ref[...]
     ).astype(jnp.bfloat16)
     inward.first(0)
+    outward.first(0)
     pools[0:16, :] = jnp.zeros((16, width), jnp.bfloat16)
     keys[...] = jnp.zeros_like(keys)
     values[...] = jnp.zeros_like(values)
-    own_sends(0)
+    each_place(begin)
 
     def table(index, carry):
         rows = block(index, row_count)
@@ -530,11 +587,12 @@
         )
 
     projected = [pick([row[i] for row in PROJECTED], z) for i in range(places)]
-    finished = [pick([row[i] for row in FINISHED], z) for i in range(places)]
+    late = [pick([row[i] for row in LATE], z) for i in range(2)]
+    finished = [pick([row[i] for row in FINISHED], z) for i in range(places * PARTS)]
 
     def project(index):
-        for p in range(PIECES):
-            share(index, mate, p).wait_recv()
+        theirs = rows_all.at[block(2 * index + mate, half_rows), :]
+        remote(theirs, theirs, token_send.at[2], mate_recv.at[index], {"tp": mate}).wait_recv()
         rows = block(index, row_count)
         normed = rows_all[rows, :]
         cosine = cos_ref[rows, :]
@@ -556,40 +614,22 @@
             keys[rows, part] = turned(raw[:, part], cosine, sine)
         values[rows, :] = product(3)
 
+    upper = z >= places // 2
+
     def project_early(i, carry):
         project(jnp.where(i == 0, projected[0], projected[1]))
         return carry
 
-    inward.first(1)
-    own_sends(1)
-    inward.second(0)
-    inward.first(2)
-    for d in range(1, places):
-        outward.start(d)
-    own_sends(2)
-    inward.second(1)
-    inward.first(3)
-    inward.second(2)
-    taken((1, 0, 3, 2))
-    inward.second(3)
-    outward.first(0)
-    outward.first(1)
-    taken((None, 2, None, None))
-    for d in range(places):
-        inward.third(d)
-    outward.first(2)
-    outward.first(3)
+    each_place(gather)
     lax.fori_loop(0, 2, project_early, 0)
-    outward.second(0)
-    taken((2, None, 0, 0))
-    outward.second(1)
-    outward.second(2)
-    project(projected[2])
-    outward.second(3)
-    taken((None, 3, 1, None))
+    each_place(relay)
+
+    @pl.when(upper)
+    def _():
+        project(projected[2])
+
+    each_place(finish_gather)
     map_in.wait()
-    for d in range(places):
-        outward.third(d)
 
     level = lax.rem(c * map_ref.shape[0] + z, 4)
     window = jnp.where(
@@ -603,7 +643,7 @@
         return remote(
             to_mate.at[step],
             from_mate.at[step],
-            half_send.at[step],
+            half_send.at[0],
             half_recv.at[step],
             {"tp": mate},
         )
@@ -618,7 +658,7 @@
         return remote(
             to_peer.at[to * PARTS + h],
             merging.at[crossing(to, h)],
-            merge_send.at[crossing(to, h)],
+            peer_send.at[0],
             merge_recv.at[crossing(to, h)],
             {"sp": pair},
         )
@@ -627,7 +667,7 @@
         return remote(
             to_peer.at[to * PARTS + h],
             from_peer.at[h],
-            peer_send.at[crossing(to, h)],
+            peer_send.at[0],
             peer_recv.at[h],
             {"sp": to},
         )
@@ -636,17 +676,16 @@
         return remote(
             to_peer.at[pair * PARTS + h],
             from_peer.at[PARTS + h],
-            peer_send.at[2 * PARTS + h],
+            peer_send.at[0],
             peer_recv.at[PARTS + h],
             {"sp": pair},
         )
 
     def step_place(step):
-        turn = step // PARTS
-        to = finished[places - 1]
-        for i in range(places - 1):
-            to = jnp.where(turn == i, finished[i], to)
-        return to, lax.rem(step, PARTS)
+        slot = finished[0]
+        for i in range(1, places * PARTS):
+            slot = jnp.where(step == i, finished[i], slot)
+        return slot // PARTS, lax.rem(slot, PARTS)
 
     def compute(step):
         to, h = step_place(step)
@@ -732,7 +771,7 @@
 
     def merge(turn):
         place = turn // PARTS
-        to = jnp.where(z < places // 2, places - 1 - place, place)
+        to = jnp.where(upper, place, places // 2 + place)
         h = lax.rem(turn, PARTS)
         to_inner(to, h).wait_recv()
         to_peer[to * PARTS + h] = (
@@ -743,20 +782,35 @@
     upper_inner = z == places // 2
 
     def body(step, carry):
-        @pl.when(step == PARTS)
-        def _():
-            taken((3, None, None, 1))
-            project(projected[3])
-
-        compute(step)
-
-        @pl.when(step > 0)
+        grows = (step == late[0]) | (step == late[1])
+
+        @pl.when(grows)
         def _():
             finish(step - 1)
 
-        @pl.when(upper_inner & (step > 2) & (lax.rem(step, 2) == 1))
+            @pl.when((z == 0) & (step == late[0]))
+            def _():
+                take(0, 2)
+
+            @pl.when((z == 0) & (step == late[1]))
+            def _():
+                take(0, 3)
+
+            @pl.when(z == places - 1)
+            def _():
+                take(places - 1, 1)
+
+            project(jnp.where(step == late[1], projected[3], projected[2]))
+
+        compute(step)
+
+        @pl.when(jnp.logical_not(grows) & (step > 0))
         def _():
-            merge((step - 3) // 2)
+            finish(step - 1)
+
+        @pl.when(upper_inner & (step == 5))
+        def _():
+            merge(0)
 
         return carry
 
@@ -767,13 +821,9 @@
         merge(turn)
         return carry
 
-    @pl.when(z == places // 2 - 1)
+    @pl.when(jnp.logical_not(outer))
     def _():
-        lax.fori_loop(0, 2 * PARTS, merge_more, 0)
-
-    @pl.when(upper_inner)
-    def _():
-        merge(2 * PARTS - 1)
+        lax.fori_loop(jnp.where(upper, 1, 0), 2 * PARTS, merge_more, 0)
 
     for h in range(PARTS):
         to_pair(h).wait_recv()
@@ -787,25 +837,16 @@
     outward.drain()
 
     def drain(place):
-        for b in range(places):
-            for p in range(PIECES):
-                if b <= place < places - 1:
-                    right(b, p).wait_send()
-                if b >= place > 0:
-                    left(b, p).wait_send()
-                share(b, c, p).wait_send()
-        for h in range(PARTS):
-            to_pair(h).wait_send()
-            for to in range(places):
-                if to // 2 != place // 2:
-                    if place in (0, places - 1):
-                        to_inner(to, h).wait_send()
-                    else:
-                        to_place(to, h).wait_send()
+        if place < places - 1:
+            sent_tokens(0, place + 1).wait_send()
+        if place > 0:
+            sent_tokens(1, places - place).wait_send()
 
     each_place(drain)
-    for step in range(places * PARTS):
-        to_sibling(step).wait_send()
+    sent_tokens(2, places).wait_send()
+    remote(to_mate, from_mate, half_send.at[0], half_recv.at[0], {"tp": mate}).wait_send()
+    sent = to_peer.at[pl.ds(0, (places - 1) * PARTS)]
+    remote(sent, sent, peer_send.at[0], peer_recv.at[0], {"sp": pair}).wait_send()
 
 
 def fused(
@@ -842,12 +883,11 @@
     def gather_sems(count):
         return [
             dma((count,)),
-            dma((places, count)),
-            dma((places, count)),
-            dma((2, 2 * places)),
-            dma((2, 2 * places)),
+            dma((places,)),
+            dma((places,)),
+            dma((2,)),
             dma((2, places)),
-            dma((2, places)),
+            dma((1,)),
         ]
 
     out = pl.pallas_call(
@@ -878,16 +918,12 @@
             dma((2,)),
             *gather_sems(4),
             *gather_sems(2),
+            dma((3,)),
             dma((places, PIECES)),
-            dma((places, PIECES)),
-            dma((places, PIECES)),
-            dma((places, PIECES)),
-            dma((places, PIECES)),
-            dma((places, PIECES)),
+            dma((places,)),
+            dma((1,)),
             dma((places * PARTS,)),
-            dma((places * PARTS,)),
-            dma((3 * PARTS,)),
-            dma((2 * PARTS,)),
+            dma((1,)),
             dma((2 * PARTS,)),
             dma((2 * PARTS,)),
         ],

time: 117 us -> 107 us (0.915)
  the two profiles are of different devices: /device:TPU:16 before, /device:TPU:25 now
where the time goes in v2:
time: 107 us
  Pallas kernels  105 us (98%)
  local copies, waits for them, and re-layouts  1.87 us (2%)
    pallas_call x1, Pallas kernels, fused(): pl.pallas_call(lambda *refs: fused_kernel(places, groups, *refs), out_sha...  105 us

profile of v2, /device:TPU:25, one launch (start us, length us, event | category | flops | bytes accessed | tf_op | source)
XLA Modules:
  0.0 106.9 jit_solution(17877835967566991847)
XLA Ops:
  0.0 105.0 %shard_map.127 = bf16[256,1024]{1,0:T(8,128)(2,1)} custom-call(bf16[256,2048]{1,0:T(8,128)(2,1)} %bitcast.6, f32[1,2048]{1,0:T(1,128)} %bitcast.7, f32[1,128]{1,0:T(1,128)} %constant.2.clone.refs_2_, bf16[128,1024]{1,0:T(8,128)(2,1)} %refs_3_.1, bf16[128,1024]{1,0:T(8,128)(2,1)} %refs_4_.1, bf16[128,1024]{1,0:T(8,128)(2,1)} %refs_5_.1, ...), custom_call_target="tpu_custom_call" | custom-call | tf_op jit(solution)/shard_map/pallas_call | solution.py:893
  105.0 1.9 %copy.15 = bf16[1,256,1024]{2,1,0:T(8,128)(2,1)} copy(bf16[1,256,1024]{2,1,0:T(8,128)(2,1)} %bitcast.5) | data formatting | bytes 1048576

commit v3 on v2

--- a/solution.py
+++ b/solution.py
@@ -193,14 +193,15 @@
 PIECES = 4
 PARTS = 2
 
-PROJECTED = ((0, 1, 2, 3), (1, 0, 2, 3), (2, 3, 0, 1), (3, 2, 0, 1))
-LATE = ((1, 3), (2, 4), (-1, 2), (-1, 2))
+PROJECTED = ((0, 1, 2, 3), (1, 0, 2, 3), (2, 0, 3, 1), (3, 0, 2, 1))
+LATE = ((1, 3), (2, 6), (2, 2), (2, 2))
 FINISHED = (
     (2, 4, 5, 6, 7, 3, 0, 1),
-    (2, 3, 4, 5, 6, 7, 0, 1),
-    (0, 1, 2, 3, 6, 7, 4, 5),
+    (2, 3, 4, 5, 0, 1, 6, 7),
+    (0, 1, 6, 7, 2, 3, 4, 5),
     (0, 1, 2, 3, 4, 5, 6, 7),
 )
+EARLY = (3, 2, 2, 2)
 ARRIVALS = ((0, 1, 2, 3), (1, 0, 3, 2), (2, 3, 0, 1), (3, 2, 1, 0))
 SENDS = ((0, 1, 2, 3), (1, 3, 2, 0), (2, 0, 1, 3), (3, 2, 1, 0))
 SLOTS = tuple(
@@ -243,6 +244,7 @@
     keys,
     values,
     pools,
+    features,
     mine,
     to_mate,
     from_mate,
@@ -356,7 +358,7 @@
                 view,
                 view,
                 self.n_send.at[side],
-                self.n_recv.at[side, d] if early else self.rest.at[0],
+                self.n_recv.at[side, d] if early else self.rest.at[d // 2],
                 {"fs": (fx, fy)[side]},
             )
 
@@ -364,7 +366,7 @@
             start, size = (self.high, self.low)[side]
             view = self.view(source[d], column, start, size)
             return remote(
-                view, view, self.n_send.at[side], self.rest.at[0], {"fs": (fx, fy)[side]}
+                view, view, self.n_send.at[side], self.rest.at[d // 2], {"fs": (fx, fy)[side]}
             )
 
         def start_own(self):
@@ -391,9 +393,9 @@
             self.near(d, 1, fy, 1).wait_recv()
             self.forward(d, 0, fy).start()
 
-        def third(self):
+        def third(self, part):
             remote(
-                self.received, self.received, self.n_send.at[0], self.rest.at[0], {"fs": fx}
+                self.received, self.received, self.n_send.at[0], self.rest.at[part], {"fs": fx}
             ).wait_recv()
 
         def drain(self):
@@ -410,7 +412,7 @@
         lambda ref, to: ref.at[:, block(to, width)],
         lambda zz, ff, m, n: weights.at[pl.ds(m, n), block(zz * groups + ff, depth), :],
         weights.at[:, pl.ds(0, filled * 3 // 8 * depth), :],
-        weights.at[:, pl.ds(0, filled // 2 * depth), :],
+        weights.at[:, pl.ds(0, filled // 4 * depth), :],
         (in_local, in_z_send, in_z_recv, in_n_send, in_n_recv, in_rest),
     )
     outward = Gather(
@@ -418,7 +420,7 @@
         lambda ref, to: ref.at[block(to, width), :],
         lambda zz, ff, m, n: outs.at[pl.ds(m, n), :, block(zz * groups + ff, out_width)],
         outs.at[:, :, pl.ds(0, filled * 3 // 8 * out_width)],
-        outs.at[:, :, pl.ds(0, filled // 2 * out_width)],
+        outs.at[:, :, pl.ds(0, filled // 4 * out_width)],
         (out_local, out_z_send, out_z_recv, out_n_send, out_n_recv, out_rest),
     )
 
@@ -447,8 +449,8 @@
         for place in range(places):
             pl.when(z == place)(lambda place=place: act(place))
 
-    def send_right(place):
-        for p in range(PIECES):
+    def send_right(place, pieces=range(PIECES)):
+        for p in pieces:
             right(place, p).start()
 
     def send_left(place):
@@ -472,46 +474,65 @@
     def prepare(place):
         for d in range(1, places):
             inward.start(d)
-        for d in range(1, places) if place in (1, 2) else (1,):
+        for d in range(1, 2 if place == 0 else places):
             outward.start(d)
 
     def begin(place):
         if place == 0:
             send_right(place)
+            for d in range(2, places):
+                outward.start(d)
         if place == places - 1:
             send_left(place)
-        if place in (0, places - 1):
-            for d in range(2, places):
-                outward.start(d)
         for p in range(PIECES):
             share(place, c, p).start()
 
     def gather(place):
-        taken = (1, 0, 3, 2)[place]
         inward.second(0)
         outward.second(0)
         inward.first(1)
         inward.first(2)
-        if place in (1, 2):
-            if place == 1:
-                send_left(place)
-            else:
-                send_right(place)
-                send_left(place)
+        if place == 0:
+            inward.second(1)
+            inward.first(3)
+            inward.second(2)
+            inward.second(3)
+            outward.first(1)
+            outward.first(2)
+            take(place, 1)
+        if place == 1:
+            send_left(place)
             inward.second(1)
             outward.first(1)
             inward.second(2)
-            take(place, taken, first_half)
+            take(place, 0, first_half)
             inward.first(3)
             outward.first(3)
-            take(place, taken, second_half)
-            if place == 1:
-                send_right(place)
+            take(place, 0, second_half)
+            send_right(place)
             outward.second(1)
             inward.second(3)
             outward.first(2)
-            take(place, (None, 2, 0, None)[place], first_half)
-        else:
+            take(place, 2, first_half)
+            outward.second(3)
+            take(place, 2, second_half)
+        if place == 2:
+            send_right(place)
+            send_left(place)
+            inward.second(1)
+            outward.first(1)
+            inward.second(2)
+            inward.first(3)
+            outward.first(3)
+            outward.second(1)
+            take(place, 3, first_half)
+            inward.second(3)
+            take(place, 3, second_half)
+            take(place, 0, first_half)
+            outward.second(3)
+            outward.first(2)
+            take(place, 0, second_half)
+        if place == 3:
             inward.second(1)
             inward.first(3)
             outward.first(1)
@@ -519,27 +540,32 @@
             outward.first(2)
             inward.second(3)
             outward.second(1)
-            take(place, taken)
             outward.first(3)
-        inward.third()
+            take(place, 2)
+            outward.second(2)
+        inward.third(0)
+        inward.third(1)
+
+    def more(place):
+        if place == 0:
+            outward.second(1)
+            outward.first(3)
+        if place in (1, 2):
+            outward.second(2)
+        if place == 3:
+            outward.second(3)
+            take(place, 0)
 
     def relay(place):
+        if place == 0:
+            outward.second(2)
         if place in (1, 2):
-            take(place, (None, 2, 0, None)[place], second_half)
-            outward.second(3)
-            outward.second(2)
-        else:
-            outward.second(2)
-            outward.second(3)
-        if place == 3:
-            take(place, 0)
+            take(place, (None, 3, 1, None)[place], first_half)
 
     def finish_gather(place):
         if place in (1, 2):
-            take(place, (None, 3, 1, None)[place], first_half)
-        outward.third()
-        if place in (1, 2):
             take(place, (None, 3, 1, None)[place], second_half)
+        outward.third(1)
 
     tokens_in = pltpu.make_async_copy(
         tokens_ref.at[block(c, half_rows), :], own_tokens, own_sem.at[0]
@@ -616,20 +642,14 @@
 
     upper = z >= places // 2
 
-    def project_early(i, carry):
-        project(jnp.where(i == 0, projected[0], projected[1]))
-        return carry
-
     each_place(gather)
-    lax.fori_loop(0, 2, project_early, 0)
+    project(projected[0])
+    each_place(more)
+    project(projected[1])
     each_place(relay)
 
-    @pl.when(upper)
-    def _():
-        project(projected[2])
-
-    each_place(finish_gather)
     map_in.wait()
+    outward.third(0)
 
     level = lax.rem(c * map_ref.shape[0] + z, 4)
     window = jnp.where(
@@ -734,15 +754,23 @@
             jnp.dot(mixed, own_map[...], preferred_element_type=jnp.float32) * scale_ref[z]
         ).astype(jnp.bfloat16)
 
-        def partial_of(side):
-            columns = block(side, half_out)
-            return jnp.dot(
-                pooled, outs[0, :, columns], preferred_element_type=jnp.float32
-            ) + jnp.dot(attn, outs[1, :, columns], preferred_element_type=jnp.float32)
-
-        to_mate[step] = partial_of(mate).astype(jnp.bfloat16)
-        to_sibling(step).start()
-        mine[lax.rem(step, 2)] = partial_of(c)
+        features[step] = jnp.concatenate([pooled, attn], 1)
+        return pooled, attn
+
+    def partial_of(step, pooled, attn, side):
+        columns = block(side, half_out)
+        value = jnp.dot(
+            pooled, outs[0, :, columns], preferred_element_type=jnp.float32
+        ) + jnp.dot(attn, outs[1, :, columns], preferred_element_type=jnp.float32)
+
+        @pl.when(side == c)
+        def _():
+            mine[lax.rem(step, 2)] = value
+
+        @pl.when(side != c)
+        def _():
+            to_mate[step] = value.astype(jnp.bfloat16)
+            to_sibling(step).start()
 
     def finish(step):
         to, h = step_place(step)
@@ -779,51 +807,96 @@
         ).astype(jnp.bfloat16)
         to_place(to, h).start()
 
-    upper_inner = z == places // 2
-
-    def body(step, carry):
-        grows = (step == late[0]) | (step == late[1])
-
-        @pl.when(grows)
+    side = z // (places // 2)
+    eager = side == c
+    early = pick(EARLY, z)
+    merged = jnp.where(upper, jnp.where(eager, 3, 4), jnp.where(eager, 5, places * PARTS))
+
+    def grow(step):
+        @pl.when((step == late[0]) | (step == late[1]))
         def _():
-            finish(step - 1)
-
             @pl.when((z == 0) & (step == late[0]))
             def _():
+                outward.second(3)
                 take(0, 2)
 
             @pl.when((z == 0) & (step == late[1]))
             def _():
                 take(0, 3)
 
-            @pl.when(z == places - 1)
+            @pl.when((z == places - 1) & (step == late[0]))
             def _():
                 take(places - 1, 1)
 
-            project(jnp.where(step == late[1], projected[3], projected[2]))
-
-        compute(step)
-
-        @pl.when(jnp.logical_not(grows) & (step > 0))
+            def project_late(i, carry):
+                project(jnp.where(i == 2, projected[2], projected[3]))
+                return carry
+
+            lax.fori_loop(
+                jnp.where(step == late[0], 2, 3), jnp.where(step == late[1], 4, 3), project_late, 0
+            )
+
+    def first_side(step, carry):
+        grow(step)
+        partial_of(step, *compute(step), side)
+
+        @pl.when(eager & (step > 0))
         def _():
             finish(step - 1)
 
-        @pl.when(upper_inner & (step == 5))
+        return carry
+
+    def second_side(step):
+        pooled, attn = features[step, :, :width], features[step, :, width:]
+        partial_of(step, pooled, attn, 1 - side)
+
+    def other_side(step, carry):
+        second_side(step)
+
+        @pl.when(jnp.logical_not(eager) & (step > 0))
         def _():
-            merge(0)
+            finish(step - 1)
 
         return carry
 
-    lax.fori_loop(0, places * PARTS, body, 0)
-    finish(places * PARTS - 1)
+    def both_sides(step, carry):
+        grow(step)
+        partial_of(step, *compute(step), side)
+        second_side(step)
+
+        @pl.when(step > early)
+        def _():
+            finish(step - 1)
+
+        @pl.when(jnp.logical_not(outer) & ((step == merged) | (step == merged + 1)))
+        def _():
+            merge(step - merged)
+
+        return carry
+
+    lax.fori_loop(0, early, first_side, 0)
+
+    @pl.when(eager)
+    def _():
+        finish(early - 1)
+
+    each_place(finish_gather)
+    lax.fori_loop(0, early, other_side, 0)
+
+    @pl.when(jnp.logical_not(eager))
+    def _():
+        finish(early - 1)
 
     def merge_more(turn, carry):
         merge(turn)
         return carry
 
+    lax.fori_loop(early, places * PARTS, both_sides, 0)
+    finish(places * PARTS - 1)
+
     @pl.when(jnp.logical_not(outer))
     def _():
-        lax.fori_loop(jnp.where(upper, 1, 0), 2 * PARTS, merge_more, 0)
+        lax.fori_loop(jnp.where(upper | eager, PARTS, 0), 2 * PARTS, merge_more, 0)
 
     for h in range(PARTS):
         to_pair(h).wait_recv()
@@ -887,7 +960,7 @@
             dma((places,)),
             dma((2,)),
             dma((2, places)),
-            dma((1,)),
+            dma((2,)),
         ]
 
     out = pl.pallas_call(
@@ -907,6 +980,7 @@
             pltpu.VMEM((length, GROUP_DIM), low),
             pltpu.VMEM((length, GROUP_DIM), low),
             pltpu.VMEM((length + 16, GROUP_DIM), low),
+            pltpu.VMEM((places * PARTS, row_count // PARTS, 2 * GROUP_DIM), low),
             pltpu.VMEM((2, row_count // PARTS, half_out), jnp.float32),
             pltpu.VMEM((places * PARTS, row_count // PARTS, half_out), low),
             pltpu.VMEM((places * PARTS, row_count // PARTS, half_out), low),

time: 107 us -> 101 us (0.944)
  the two profiles are of different devices: /device:TPU:25 before, /device:TPU:16 now
where the time goes in v3:
time: 101 us
  Pallas kernels  99.1 us (98%)
  local copies, waits for them, and re-layouts  1.87 us (2%)
    pallas_call x1, Pallas kernels, fused(): pl.pallas_call(lambda *refs: fused_kernel(places, groups, *refs), out_sha...  99.1 us

profile of v3, /device:TPU:16, one launch (start us, length us, event | category | flops | bytes accessed | tf_op | source)
XLA Modules:
  0.0 101.0 jit_solution(11965257167605912684)
XLA Ops:
  0.0 99.1 %shard_map.127 = bf16[256,1024]{1,0:T(8,128)(2,1)} custom-call(bf16[256,2048]{1,0:T(8,128)(2,1)} %bitcast.6, f32[1,2048]{1,0:T(1,128)} %bitcast.7, f32[1,128]{1,0:T(1,128)} %constant.2.clone.refs_2_, bf16[128,1024]{1,0:T(8,128)(2,1)} %refs_3_.1, bf16[128,1024]{1,0:T(8,128)(2,1)} %refs_4_.1, bf16[128,1024]{1,0:T(8,128)(2,1)} %refs_5_.1, ...), custom_call_target="tpu_custom_call" | custom-call | tf_op jit(solution)/shard_map/pallas_call | solution.py:966
  99.1 1.9 %copy.15 = bf16[1,256,1024]{2,1,0:T(8,128)(2,1)} copy(bf16[1,256,1024]{2,1,0:T(8,128)(2,1)} %bitcast.5) | data formatting | bytes 1048576

commit v4 on v3

--- a/solution.py
+++ b/solution.py
@@ -194,14 +194,16 @@
 PARTS = 2
 
 PROJECTED = ((0, 1, 2, 3), (1, 0, 2, 3), (2, 0, 3, 1), (3, 0, 2, 1))
-LATE = ((1, 3), (2, 6), (2, 2), (2, 2))
+LATE = ((2, 4), (0, 4), (2, 2), (2, 2))
 FINISHED = (
-    (2, 4, 5, 6, 7, 3, 0, 1),
-    (2, 3, 4, 5, 0, 1, 6, 7),
+    (2, 3, 4, 5, 6, 7, 0, 1),
+    (4, 5, 0, 1, 6, 7, 2, 3),
     (0, 1, 6, 7, 2, 3, 4, 5),
     (0, 1, 2, 3, 4, 5, 6, 7),
 )
-EARLY = (3, 2, 2, 2)
+EARLY = (4, 2, 2, 2)
+SECOND = ((2, 3, 4, 5, 0, 1, 6, 7),) + 3 * ((0, 1, 2, 3, 4, 5, 6, 7),)
+AHEAD = (2, 2, 2, 2)
 ARRIVALS = ((0, 1, 2, 3), (1, 0, 3, 2), (2, 3, 0, 1), (3, 2, 1, 0))
 SENDS = ((0, 1, 2, 3), (1, 3, 2, 0), (2, 0, 1, 3), (3, 2, 1, 0))
 SLOTS = tuple(
@@ -220,21 +222,25 @@
     places,
     groups,
     tokens_ref,
-    norm_gain_ref,
-    freqs_ref,
+    norm_gain_hbm,
+    freqs_hbm,
     pool_ref,
     query_ref,
     key_ref,
     value_ref,
     map_ref,
-    scale_ref,
-    gain_ref,
+    scale_hbm,
+    gain_hbm,
     lambda_ref,
     out_pool_ref,
     out_heads_ref,
     out_ref,
     own_tokens,
     own_map,
+    norm_gain_ref,
+    freqs_ref,
+    scale_ref,
+    gain_ref,
     cos_ref,
     sin_ref,
     rows_all,
@@ -257,6 +263,7 @@
 ):
     (
         own_sem,
+        small_sem,
         in_local,
         in_z_send,
         in_z_recv,
@@ -299,6 +306,17 @@
     def block(index, size):
         return pl.ds(pl.multiple_of(index * size, size), size)
 
+    small = [
+        pltpu.make_async_copy(source, target, small_sem.at[i])
+        for i, (source, target) in enumerate(
+            (
+                (norm_gain_hbm, norm_gain_ref),
+                (freqs_hbm, freqs_ref),
+                (scale_hbm, scale_ref),
+                (gain_hbm, gain_ref),
+            )
+        )
+    ]
     barrier = pltpu.get_barrier_semaphore()
     partners = [{"sp": lax.rem(z + d, places)} for d in range(1, places)]
     partners += [{"fs": fx}, {"fs": fy}, {"tp": mate}]
@@ -480,8 +498,6 @@
     def begin(place):
         if place == 0:
             send_right(place)
-            for d in range(2, places):
-                outward.start(d)
         if place == places - 1:
             send_left(place)
         for p in range(PIECES):
@@ -500,6 +516,9 @@
             outward.first(1)
             outward.first(2)
             take(place, 1)
+            outward.second(1)
+            for d in range(2, places):
+                outward.start(d)
         if place == 1:
             send_left(place)
             inward.second(1)
@@ -507,9 +526,9 @@
             inward.second(2)
             take(place, 0, first_half)
             inward.first(3)
-            outward.first(3)
             take(place, 0, second_half)
             send_right(place)
+            outward.first(3)
             outward.second(1)
             inward.second(3)
             outward.first(2)
@@ -525,13 +544,11 @@
             inward.first(3)
             outward.first(3)
             outward.second(1)
-            take(place, 3, first_half)
+            take(place, 0, first_half)
             inward.second(3)
-            take(place, 3, second_half)
-            take(place, 0, first_half)
+            take(place, 0, second_half)
             outward.second(3)
-            outward.first(2)
-            take(place, 0, second_half)
+            take(place, 3)
         if place == 3:
             inward.second(1)
             inward.first(3)
@@ -540,31 +557,39 @@
             outward.first(2)
             inward.second(3)
             outward.second(1)
-            outward.first(3)
             take(place, 2)
             outward.second(2)
         inward.third(0)
         inward.third(1)
 
+    def relay_piece(p):
+        def act(place):
+            if place in (1, 2):
+                take(place, (None, 3, 1, None)[place], (p,))
+
+        each_place(act)
+
     def more(place):
         if place == 0:
-            outward.second(1)
             outward.first(3)
-        if place in (1, 2):
+        if place == 1:
+            outward.second(2)
+        if place == 2:
+            outward.first(2)
+        if place == 3:
+            take(place, 0)
+
+    def relay(place):
+        if place in (0, 2):
             outward.second(2)
         if place == 3:
-            outward.second(3)
-            take(place, 0)
-
-    def relay(place):
-        if place == 0:
-            outward.second(2)
-        if place in (1, 2):
-            take(place, (None, 3, 1, None)[place], first_half)
+            outward.first(3)
 
     def finish_gather(place):
         if place in (1, 2):
-            take(place, (None, 3, 1, None)[place], second_half)
+            take(place, (None, 3, 1, None)[place], second_half[1:])
+        if place == places - 1:
+            outward.second(3)
         outward.third(1)
 
     tokens_in = pltpu.make_async_copy(
@@ -572,12 +597,16 @@
     )
     map_in = pltpu.make_async_copy(map_ref.at[z], own_map, own_sem.at[1])
     tokens_in.start()
+    for copy in small:
+        copy.start()
     inward.start_own()
     outward.start_own()
     map_in.start()
     pl.semaphore_wait(barrier, len(partners))
     each_place(prepare)
     tokens_in.wait()
+    for copy in small:
+        copy.wait()
     floated = own_tokens[...].astype(jnp.float32)
     rows_all[block(2 * z + c, half_rows), :] = (
         floated
@@ -645,8 +674,10 @@
     each_place(gather)
     project(projected[0])
     each_place(more)
+    relay_piece(0)
     project(projected[1])
     each_place(relay)
+    relay_piece(1)
 
     map_in.wait()
     outward.third(0)
@@ -757,7 +788,7 @@
         features[step] = jnp.concatenate([pooled, attn], 1)
         return pooled, attn
 
-    def partial_of(step, pooled, attn, side):
+    def partial_of(step, turn, pooled, attn, side):
         columns = block(side, half_out)
         value = jnp.dot(
             pooled, outs[0, :, columns], preferred_element_type=jnp.float32
@@ -765,19 +796,19 @@
 
         @pl.when(side == c)
         def _():
-            mine[lax.rem(step, 2)] = value
+            mine[lax.rem(turn, 2)] = value
 
         @pl.when(side != c)
         def _():
             to_mate[step] = value.astype(jnp.bfloat16)
             to_sibling(step).start()
 
-    def finish(step):
+    def finish(step, turn):
         to, h = step_place(step)
         slot = to * PARTS + h
         crosses = to // 2 != z // 2
         to_sibling(step).wait_recv()
-        summed = mine[lax.rem(step, 2)] + from_mate[step].astype(jnp.float32)
+        summed = mine[lax.rem(turn, 2)] + from_mate[step].astype(jnp.float32)
 
         @pl.when(to == z)
         def _():
@@ -810,7 +841,8 @@
     side = z // (places // 2)
     eager = side == c
     early = pick(EARLY, z)
-    merged = jnp.where(upper, jnp.where(eager, 3, 4), jnp.where(eager, 5, places * PARTS))
+    merged = jnp.where(upper, jnp.where(eager, 2, 3), jnp.where(eager, 3, 5))
+    lag = jnp.where(outer, 0, 1)
 
     def grow(step):
         @pl.when((step == late[0]) | (step == late[1]))
@@ -824,11 +856,11 @@
             def _():
                 take(0, 3)
 
-            @pl.when((z == places - 1) & (step == late[0]))
-            def _():
-                take(places - 1, 1)
-
             def project_late(i, carry):
+                @pl.when((z == places - 1) & (i == 3))
+                def _():
+                    take(places - 1, 1)
+
                 project(jnp.where(i == 2, projected[2], projected[3]))
                 return carry
 
@@ -836,67 +868,103 @@
                 jnp.where(step == late[0], 2, 3), jnp.where(step == late[1], 4, 3), project_late, 0
             )
 
+    ahead = pick(AHEAD, z)
+    last = places * PARTS - 1
+    seconds = [pick([row[i] for row in SECOND], z) for i in range(places * PARTS)]
+
+    def second_step(turn):
+        step = seconds[0]
+        for i in range(1, places * PARTS):
+            step = jnp.where(turn == i, seconds[i], step)
+        return step
+
     def first_side(step, carry):
         grow(step)
-        partial_of(step, *compute(step), side)
-
-        @pl.when(eager & (step > 0))
-        def _():
-            finish(step - 1)
+
+        @pl.when(step == 1)
+        def _():
+            relay_piece(2)
+
+        partial_of(step, step, *compute(step), side)
+
+        @pl.when(eager & (step >= lag))
+        def _():
+            finish(step - lag, step - lag)
 
         return carry
 
-    def second_side(step):
+    def second_side(turn):
+        step = second_step(turn)
         pooled, attn = features[step, :, :width], features[step, :, width:]
-        partial_of(step, pooled, attn, 1 - side)
-
-    def other_side(step, carry):
-        second_side(step)
-
-        @pl.when(jnp.logical_not(eager) & (step > 0))
-        def _():
-            finish(step - 1)
+        partial_of(step, turn, pooled, attn, 1 - side)
+
+    def other_side(turn, carry):
+        second_side(turn)
+
+        @pl.when(jnp.logical_not(eager) & (turn > 0))
+        def _():
+            finish(second_step(turn - 1), turn - 1)
 
         return carry
 
     def both_sides(step, carry):
         grow(step)
-        partial_of(step, *compute(step), side)
-        second_side(step)
-
-        @pl.when(step > early)
-        def _():
-            finish(step - 1)
-
-        @pl.when(jnp.logical_not(outer) & ((step == merged) | (step == merged + 1)))
-        def _():
-            merge(step - merged)
+        partial_of(step, step, *compute(step), side)
+        at_once = eager & outer & (step == early)
+
+        @pl.when(at_once)
+        def _():
+            finish(step, step)
+
+        second_side(step - early + ahead)
+
+        @pl.when((step != early + 1 - lag) & jnp.logical_not(at_once))
+        def _():
+            first = jnp.where(step == early, step, step - 1)
+            turn = first - early + ahead
+            finish(jnp.where(eager, first, second_step(turn)), jnp.where(eager, first, turn))
+
+        again = upper & (step == last)
+
+        @pl.when(jnp.logical_not(outer) & ((step == merged) | (step == merged + 1) | again))
+        def _():
+            merge(jnp.where(again, PARTS, step - merged))
 
         return carry
 
     lax.fori_loop(0, early, first_side, 0)
-
-    @pl.when(eager)
+    each_place(finish_gather)
+
+    @pl.when(eager & jnp.logical_not(outer))
     def _():
-        finish(early - 1)
-
-    each_place(finish_gather)
-    lax.fori_loop(0, early, other_side, 0)
+        finish(early - 1, early - 1)
+
+    lax.fori_loop(0, ahead, other_side, 0)
 
     @pl.when(jnp.logical_not(eager))
     def _():
-        finish(early - 1)
+        finish(second_step(ahead - 1), ahead - 1)
 
     def merge_more(turn, carry):
         merge(turn)
         return carry
 
     lax.fori_loop(early, places * PARTS, both_sides, 0)
-    finish(places * PARTS - 1)
+    def second_more(turn, carry):
+        second_side(turn)
+
+        @pl.when(jnp.logical_not(eager))
+        def _():
+            finish(second_step(turn - 1), turn - 1)
+
+        return carry
+
+    lax.fori_loop(last + 1 - early + ahead, last + 1, second_more, 0)
+    finish(jnp.where(eager, last, second_step(last)), last)
 
     @pl.when(jnp.logical_not(outer))
     def _():
-        lax.fori_loop(jnp.where(upper | eager, PARTS, 0), 2 * PARTS, merge_more, 0)
+        lax.fori_loop(jnp.where(upper, PARTS + 1, PARTS), 2 * PARTS, merge_more, 0)
 
     for h in range(PARTS):
         to_pair(h).wait_recv()
@@ -966,11 +1034,15 @@
     out = pl.pallas_call(
         lambda *refs: fused_kernel(places, groups, *refs),
         out_shape=jax.ShapeDtypeStruct((row_count, half_out), low),
-        in_specs=[hbm, vmem, vmem] + [hbm] * 5 + [vmem] * 2 + [smem] + [hbm] * 2,
+        in_specs=[hbm] * 10 + [smem] + [hbm] * 2,
         out_specs=vmem,
         scratch_shapes=[
             pltpu.VMEM((row_count // 2, model), low),
             pltpu.VMEM((GROUP_DIM, GROUP_DIM), low),
+            pltpu.VMEM((1, model), jnp.float32),
+            pltpu.VMEM((1, HEAD_DIM), jnp.float32),
+            pltpu.VMEM((group_count, 1, GROUP_DIM), jnp.float32),
+            pltpu.VMEM((1, 2 * HEAD_DIM), jnp.float32),
             pltpu.VMEM((length, HEAD_DIM), jnp.float32),
             pltpu.VMEM((length, HEAD_DIM), jnp.float32),
             pltpu.VMEM((length, model), low),
@@ -990,6 +1062,7 @@
             pltpu.VMEM((2 * PARTS, row_count // PARTS, half_out), low),
             pltpu.VMEM((PARTS, row_count // PARTS, half_out), jnp.float32),
             dma((2,)),
+            dma((4,)),
             *gather_sems(4),
             *gather_sems(2),
             dma((3,)),

time: 101 us -> 98 us (0.970)
  Pallas kernels: 99.1 us -> 96 us
    pallas_call x1, Pallas kernels: 99.1 us -> 96 us  [fused(): pl.pallas_call(lambda *refs: fused_kernel(places, groups, *refs), out_sha...]
where the time goes in v4:
time: 98 us; the launch traced here: 97.8 us
  Pallas kernels  96 us (98%)
  local copies, waits for them, and re-layouts  1.87 us (2%)
    pallas_call x1, Pallas kernels, fused(): pl.pallas_call(lambda *refs: fused_kernel(places, groups, *refs), out_sha...  96 us

profile of v4, /device:TPU:16, one launch (start us, length us, event | category | flops | bytes accessed | tf_op | source)
XLA Modules:
  0.0 97.8 jit_solution(3458999866418821632)
XLA Ops:
  0.0 96.0 %shard_map.127 = bf16[256,1024]{1,0:T(8,128)(2,1)} custom-call(bf16[256,2048]{1,0:T(8,128)(2,1)} %bitcast.6, f32[1,2048]{1,0:T(1,128)} %bitcast.7, f32[1,128]{1,0:T(1,128)} %constant.2.clone.refs_2_, bf16[128,1024]{1,0:T(8,128)(2,1)} %refs_3_.1, bf16[128,1024]{1,0:T(8,128)(2,1)} %refs_4_.1, bf16[128,1024]{1,0:T(8,128)(2,1)} %refs_5_.1, ...), custom_call_target="tpu_custom_call" | custom-call | tf_op jit(solution)/shard_map/pallas_call | solution.py:1034
  96.0 1.9 %copy.15 = bf16[1,256,1024]{2,1,0:T(8,128)(2,1)} copy(bf16[1,256,1024]{2,1,0:T(8,128)(2,1)} %bitcast.5) | data formatting | bytes 1048576

commit v5 on v4

--- a/solution.py
+++ b/solution.py
@@ -231,7 +231,7 @@
     map_ref,
     scale_hbm,
     gain_hbm,
-    lambda_ref,
+    lambda_hbm,
     out_pool_ref,
     out_heads_ref,
     out_ref,
@@ -241,6 +241,7 @@
     freqs_ref,
     scale_ref,
     gain_ref,
+    lambda_ref,
     cos_ref,
     sin_ref,
     rows_all,
@@ -314,6 +315,7 @@
                 (freqs_hbm, freqs_ref),
                 (scale_hbm, scale_ref),
                 (gain_hbm, gain_ref),
+                (lambda_hbm, lambda_ref),
             )
         )
     ]
@@ -738,19 +740,17 @@
             slot = jnp.where(step == i, finished[i], slot)
         return slot // PARTS, lax.rem(slot, PARTS)
 
-    def compute(step):
-        to, h = step_place(step)
-        slot = to * PARTS + h
+    def attend(step, slot, span):
         rows = block(slot, part_rows)
-        query_pos = slot * part_rows + lax.broadcasted_iota(jnp.int32, (part_rows, length), 0)
-        key_pos = lax.broadcasted_iota(jnp.int32, (part_rows, length), 1)
+        query_pos = slot * part_rows + lax.broadcasted_iota(jnp.int32, (part_rows, span), 0)
+        key_pos = lax.broadcasted_iota(jnp.int32, (part_rows, span), 1)
         seen = query_pos >= key_pos
         mapped = []
         for m in range(2):
             part = slice(m * HEAD_DIM, (m + 1) * HEAD_DIM)
             scores = lax.dot_general(
                 queries[rows, part],
-                keys[:, part],
+                keys[:span, part],
                 (((1,), (1,)), ((), ())),
                 preferred_element_type=jnp.float32,
             ) * HEAD_DIM ** (-0.5)
@@ -759,7 +759,7 @@
             totals = jnp.sum(expons, -1, keepdims=True)
             mapped.append(
                 jnp.dot(
-                    expons.astype(jnp.bfloat16), values[...], preferred_element_type=jnp.float32
+                    expons.astype(jnp.bfloat16), values[:span, :], preferred_element_type=jnp.float32
                 )
                 / totals
             )
@@ -786,7 +786,14 @@
         ).astype(jnp.bfloat16)
 
         features[step] = jnp.concatenate([pooled, attn], 1)
-        return pooled, attn
+
+    def compute(step):
+        to, h = step_place(step)
+        slot = to * PARTS + h
+        half = places // 2
+        pl.when(to < half)(lambda: attend(step, slot, half * row_count))
+        pl.when(to >= half)(lambda: attend(step, slot, length))
+        return features[step, :, :width], features[step, :, width:]
 
     def partial_of(step, turn, pooled, attn, side):
         columns = block(side, half_out)
@@ -1016,7 +1023,6 @@
     group_count = pool_map.shape[0]
     half_out = model // 2
     vmem = pl.BlockSpec(memory_space=pltpu.VMEM)
-    smem = pl.BlockSpec(memory_space=pltpu.SMEM)
     hbm = pl.BlockSpec(memory_space=pl.ANY)
     dma = pltpu.SemaphoreType.DMA
     low = jnp.bfloat16
@@ -1034,7 +1040,7 @@
     out = pl.pallas_call(
         lambda *refs: fused_kernel(places, groups, *refs),
         out_shape=jax.ShapeDtypeStruct((row_count, half_out), low),
-        in_specs=[hbm] * 10 + [smem] + [hbm] * 2,
+        in_specs=[hbm] * 13,
         out_specs=vmem,
         scratch_shapes=[
             pltpu.VMEM((row_count // 2, model), low),
@@ -1043,6 +1049,7 @@
             pltpu.VMEM((1, HEAD_DIM), jnp.float32),
             pltpu.VMEM((group_count, 1, GROUP_DIM), jnp.float32),
             pltpu.VMEM((1, 2 * HEAD_DIM), jnp.float32),
+            pltpu.SMEM(diff_lambda.shape, jnp.float32),
             pltpu.VMEM((length, HEAD_DIM), jnp.float32),
             pltpu.VMEM((length, HEAD_DIM), jnp.float32),
             pltpu.VMEM((length, model), low),
@@ -1062,7 +1069,7 @@
             pltpu.VMEM((2 * PARTS, row_count // PARTS, half_out), low),
             pltpu.VMEM((PARTS, row_count // PARTS, half_out), jnp.float32),
             dma((2,)),
-            dma((4,)),
+            dma((5,)),
             *gather_sems(4),
             *gather_sems(2),
             dma((3,)),

time: 98 us -> 97 us (0.990)
  Pallas kernels: 96 us -> 95 us
where the time goes in v5:
time: 97 us; the launch traced here: 96.9 us
  Pallas kernels  95 us (98%)
  local copies, waits for them, and re-layouts  1.87 us (2%)
    pallas_call x1, Pallas kernels, fused(): pl.pallas_call(lambda *refs: fused_kernel(places, groups, *refs), out_sha...  95 us

profile of v5, /device:TPU:16, one launch (start us, length us, event | category | flops | bytes accessed | tf_op | source)
XLA Modules:
  0.0 96.9 jit_solution(15446321066441275816)
XLA Ops:
  0.0 95.0 %shard_map.127 = bf16[256,1024]{1,0:T(8,128)(2,1)} custom-call(bf16[256,2048]{1,0:T(8,128)(2,1)} %bitcast.6, f32[1,2048]{1,0:T(1,128)} %bitcast.7, f32[1,128]{1,0:T(1,128)} %constant.2.clone.refs_2_, bf16[128,1024]{1,0:T(8,128)(2,1)} %refs_3_.1, bf16[128,1024]{1,0:T(8,128)(2,1)} %refs_4_.1, bf16[128,1024]{1,0:T(8,128)(2,1)} %refs_5_.1, ...), custom_call_target="tpu_custom_call" | custom-call | tf_op jit(solution)/shard_map/pallas_call | solution.py:1040
  95.0 1.9 %copy.15 = bf16[1,256,1024]{2,1,0:T(8,128)(2,1)} copy(bf16[1,256,1024]{2,1,0:T(8,128)(2,1)} %bitcast.5) | data formatting | bytes 1048576

commit v6 on v5

--- a/solution.py
+++ b/solution.py
@@ -190,7 +190,7 @@
 
 
 MESH = pl.DeviceIdType.MESH
-PIECES = 4
+PIECES = 8
 PARTS = 2
 
 PROJECTED = ((0, 1, 2, 3), (1, 0, 2, 3), (2, 0, 3, 1), (3, 0, 2, 1))
@@ -567,7 +567,7 @@
     def relay_piece(p):
         def act(place):
             if place in (1, 2):
-                take(place, (None, 3, 1, None)[place], (p,))
+                take(place, (None, 3, 1, None)[place], range(p * PIECES // 4, (p + 1) * PIECES // 4))
 
         each_place(act)
 
@@ -589,7 +589,7 @@
 
     def finish_gather(place):
         if place in (1, 2):
-            take(place, (None, 3, 1, None)[place], second_half[1:])
+            take(place, (None, 3, 1, None)[place], range(3 * PIECES // 4, PIECES))
         if place == places - 1:
             outward.second(3)
         outward.third(1)

time: 97 us -> 96.1 us (level)
  Pallas kernels: 95 us -> 94 us
where the time goes in v6:
time: 96.1 us; the launch traced here: 95.9 us
  Pallas kernels  94 us (98%)
  local copies, waits for them, and re-layouts  1.87 us (2%)
    pallas_call x1, Pallas kernels, fused(): pl.pallas_call(lambda *refs: fused_kernel(places, groups, *refs), out_sha...  94 us

profile of v6, /device:TPU:16, one launch (start us, length us, event | category | flops | bytes accessed | tf_op | source)
XLA Modules:
  0.0 95.9 jit_solution(11145320770736520645)
XLA Ops:
  0.0 94.0 %shard_map.127 = bf16[256,1024]{1,0:T(8,128)(2,1)} custom-call(bf16[256,2048]{1,0:T(8,128)(2,1)} %bitcast.6, f32[1,2048]{1,0:T(1,128)} %bitcast.7, f32[1,128]{1,0:T(1,128)} %constant.2.clone.refs_2_, bf16[128,1024]{1,0:T(8,128)(2,1)} %refs_3_.1, bf16[128,1024]{1,0:T(8,128)(2,1)} %refs_4_.1, bf16[128,1024]{1,0:T(8,128)(2,1)} %refs_5_.1, ...), custom_call_target="tpu_custom_call" | custom-call | tf_op jit(solution)/shard_map/pallas_call | solution.py:1040
  94.0 1.9 %copy.15 = bf16[1,256,1024]{2,1,0:T(8,128)(2,1)} copy(bf16[1,256,1024]{2,1,0:T(8,128)(2,1)} %bitcast.5) | data formatting | bytes 1048576

commit v7 on v6

--- a/solution.py
+++ b/solution.py
@@ -260,6 +260,8 @@
     from_peer,
     merging,
     final,
+    result,
+    result_sem,
     *sems,
 ):
     (
@@ -973,16 +975,22 @@
     def _():
         lax.fori_loop(jnp.where(upper, PARTS + 1, PARTS), 2 * PARTS, merge_more, 0)
 
+    def result_out(h):
+        return pltpu.make_async_copy(
+            result.at[h], out_ref.at[pl.ds(h * part_rows, part_rows), :], result_sem.at[h]
+        )
+
     for h in range(PARTS):
         to_pair(h).wait_recv()
         total = final[h] + from_peer[PARTS + h].astype(jnp.float32)
         to_place(z, h).wait_recv()
-        out_ref[h * part_rows : (h + 1) * part_rows, :] = (
-            total + from_peer[h].astype(jnp.float32)
-        ).astype(out_ref.dtype)
+        result[h] = (total + from_peer[h].astype(jnp.float32)).astype(out_ref.dtype)
+        result_out(h).start()
 
     inward.drain()
     outward.drain()
+    for h in range(PARTS):
+        result_out(h).wait()
 
     def drain(place):
         if place < places - 1:
@@ -1022,7 +1030,6 @@
     freqs = jnp.asarray(np.concatenate([freqs, freqs])[None, :], jnp.float32)
     group_count = pool_map.shape[0]
     half_out = model // 2
-    vmem = pl.BlockSpec(memory_space=pltpu.VMEM)
     hbm = pl.BlockSpec(memory_space=pl.ANY)
     dma = pltpu.SemaphoreType.DMA
     low = jnp.bfloat16
@@ -1041,7 +1048,7 @@
         lambda *refs: fused_kernel(places, groups, *refs),
         out_shape=jax.ShapeDtypeStruct((row_count, half_out), low),
         in_specs=[hbm] * 13,
-        out_specs=vmem,
+        out_specs=hbm,
         scratch_shapes=[
             pltpu.VMEM((row_count // 2, model), low),
             pltpu.VMEM((GROUP_DIM, GROUP_DIM), low),
@@ -1068,6 +1075,8 @@
             pltpu.VMEM((2 * PARTS, row_count // PARTS, half_out), low),
             pltpu.VMEM((2 * PARTS, row_count // PARTS, half_out), low),
             pltpu.VMEM((PARTS, row_count // PARTS, half_out), jnp.float32),
+            pltpu.VMEM((PARTS, row_count // PARTS, half_out), low),
+            dma((PARTS,)),
             dma((2,)),
             dma((5,)),
             *gather_sems(4),

time: 96.1 us -> 96 us (level)
  no operation moved by 1% of the time
where the time goes in v7:
time: 96 us; the launch traced here: 95.8 us
  Pallas kernels  93.9 us (98%)
  local copies, waits for them, and re-layouts  1.87 us (2%)
    pallas_call x1, Pallas kernels, fused(): pl.pallas_call(lambda *refs: fused_kernel(places, groups, *refs), out_sha...  93.9 us

profile of v7, /device:TPU:16, one launch (start us, length us, event | category | flops | bytes accessed | tf_op | source)
XLA Modules:
  0.0 95.8 jit_solution(7086867087636712946)
XLA Ops:
  0.0 93.9 %shard_map.127 = bf16[256,1024]{1,0:T(8,128)(2,1)} custom-call(bf16[256,2048]{1,0:T(8,128)(2,1)} %bitcast.6, f32[1,2048]{1,0:T(1,128)} %bitcast.7, f32[1,128]{1,0:T(1,128)} %constant.2.clone.refs_2_, bf16[128,1024]{1,0:T(8,128)(2,1)} %refs_3_.1, bf16[128,1024]{1,0:T(8,128)(2,1)} %refs_4_.1, bf16[128,1024]{1,0:T(8,128)(2,1)} %refs_5_.1, ...), custom_call_target="tpu_custom_call" | custom-call | tf_op jit(solution)/shard_map/pallas_call | solution.py:1047
  94.0 1.9 %copy.15 = bf16[1,256,1024]{2,1,0:T(8,128)(2,1)} copy(bf16[1,256,1024]{2,1,0:T(8,128)(2,1)} %bitcast.5) | data formatting | bytes 1048576
